TPU v7x, 512 devices: a whole 4x8x8 slice. The times are simulated.
512 devices in a mesh: sp: 64 (over z, y), tp: 8 (over x, core).
Axes of the slice: x: 4, y: 8, z: 8, core: 2. Of those that a mesh axis runs over, the one named last changes fastest.
Arguments:
- tokens: bfloat16 [65536, 2048], P(('sp', 'tp')), may hold values from -6 to 6
- norm_gain: float32 [2048], replicated, may hold values from 0.1 to 1.9
- w_query: bfloat16 [2048, 1024], P('sp', 'tp'), may hold values from -0.125 to 0.125
- w_key: bfloat16 [2048, 1024], P('sp', 'tp'), may hold values from -0.125 to 0.125
- w_value: bfloat16 [2048, 1024], P('sp', 'tp'), may hold values from -0.125 to 0.125
- decay_rate: float32 [512, 8], P('sp', 'tp'), may hold values from 7.6293945e-07 to 0.1, as said below
- state_init: float32 [8, 128, 128], P('tp'), may hold values from -48 to 48
- out_gain: float32 [1024], P('tp'), may hold values from 0.1 to 1.9
- w_out: bfloat16 [1024, 2048], P('tp', 'sp'), may hold values from -0.1875 to 0.1875
Outputs:
- mixed: bfloat16 [65536, 2048], P(('sp', 'tp'))
Inputs may be any that keep to these rules, and one draw needn't show every extreme that they name: `decay_rate`: constant over each block of 128 positions.
All inputs are finite; a program needn't handle non-finite values.
Results may differ from a plain program's by a relative error of at most 0.025.
Values may be sent and summed in bfloat16 or wider, within the bound.
No kernel may reach another device: no remote copies, remote signals or barrier semaphores. Data moves between devices by JAX's collectives and lax.ppermute only.
A program may use at most 64 MiB of HBM per device.

v0:
```python
import jax
import jax.numpy as jnp
from jax import lax
from jax.experimental import pallas as pl
from jax.experimental.pallas import tpu as pltpu
from jax.sharding import Mesh
from jax.sharding import PartitionSpec as P


HEAD_DIM = 128
BLOCK = 128
SP = ("sp_0", "sp_1")
TP = ("tp_0", "tp_1")
ALL = SP + TP
EPS = 0.1
ROPE_BASE = 10000.0

MESSAGES = (8, HEAD_DIM + 8, HEAD_DIM)
VMEM = pl.BlockSpec(memory_space=pltpu.VMEM)
SMEM = pl.BlockSpec(memory_space=pltpu.SMEM)
ANY = pl.BlockSpec(memory_space=pl.ANY)
HBM = pl.BlockSpec(memory_space=pltpu.HBM)


def lines(first):
    groups = []
    for core in range(2):
        for fixed in range(8):
            for x in range(4):
                spots = [(fixed, m) if (core == 0) == first else (m, fixed) for m in range(8)]
                groups.append([((z * 8 + y) * 4 + x) * 2 + core for z, y in spots])
    return groups


def in_hbm(a):
    return pltpu.with_memory_space_constraint(a, pltpu.HBM)


def along(messages, first):
    return lax.all_to_all(messages, ALL, 0, 0, axis_index_groups=lines(first), tiled=True)


def shifted(own, d):
    n = lax.axis_size("tp_0")
    return lax.ppermute(own, "tp_0", [(i, (i + d) % n) for i in range(n)])


def swapped(v):
    return lax.ppermute(v, "tp_1", [(0, 1), (1, 0)])


def token_chunks(own, tables):
    same = [own] + [shifted(own, d) for d in (1, 2, 3)]
    same[2], *tables = lax.optimization_barrier((same[2], *tables))
    return same + [swapped(v) for v in same], *tables


def gather_kernel(*refs):
    chunks, out, sems = refs[:4], refs[4], refs[5]
    copies = [pltpu.make_async_copy(c, out.at[j], sems.at[j]) for j, c in enumerate(chunks)]
    for copy in copies:
        copy.start()
    for copy in copies:
        copy.wait()


def gathered(chunks):
    return pl.pallas_call(
        gather_kernel,
        out_shape=jax.ShapeDtypeStruct((4, *chunks[0].shape), chunks[0].dtype),
        in_specs=[ANY] * 4,
        out_specs=VMEM,
        scratch_shapes=[pltpu.SemaphoreType.DMA((4,))],
        compiler_params=pltpu.CompilerParams(vmem_limit_bytes=4 << 20),
        cost_estimate=pl.CostEstimate(flops=1000, bytes_accessed=4 << 20, transcendentals=0),
    )(*chunks)


def late_chunks(own):
    same = [own] + [shifted(own, d) for d in (1, 2, 3)]
    same = gathered([in_hbm(c) for c in same])
    return same, swapped(same)


def norm_kernel(x_hbm, gain_hbm, out_ref, x_ref, gain_ref, sems):
    copies = [
        pltpu.make_async_copy(x_hbm, x_ref, sems.at[0]),
        pltpu.make_async_copy(gain_hbm, gain_ref, sems.at[1]),
    ]
    for copy in copies:
        copy.start()
    for copy in copies:
        copy.wait()
    x = x_ref[...].astype(jnp.float32)
    scale = lax.rsqrt(jnp.mean(x * x, axis=-1, keepdims=True) + EPS)
    out_ref[...] = (x * scale * gain_ref[...]).astype(jnp.bfloat16)


def normalized(tokens, gain):
    return pl.pallas_call(
        norm_kernel,
        out_shape=jax.ShapeDtypeStruct(tokens.shape, jnp.bfloat16),
        in_specs=[ANY, ANY],
        out_specs=VMEM,
        scratch_shapes=[
            pltpu.VMEM(tokens.shape, tokens.dtype),
            pltpu.VMEM((1, tokens.shape[1]), gain.dtype),
            pltpu.SemaphoreType.DMA((2,)),
        ],
        compiler_params=pltpu.CompilerParams(vmem_limit_bytes=8 << 20),
        cost_estimate=pl.CostEstimate(flops=2000000, bytes_accessed=1 << 20, transcendentals=0),
    )(in_hbm(tokens), in_hbm(gain[None]))


def write_message(out, state, decay):
    row = lax.broadcasted_iota(jnp.int32, (8, HEAD_DIM), 0)
    high = decay.astype(jnp.bfloat16).astype(jnp.float32)
    rest = decay - high
    middle = rest.astype(jnp.bfloat16).astype(jnp.float32)
    addends = jnp.where(row == 0, high, jnp.where(row == 1, middle, rest - middle))
    addends = jnp.where(row < 3, addends, 0.0).astype(jnp.bfloat16)
    state = state.astype(jnp.bfloat16)
    for i in range(8):
        out[i, 0:HEAD_DIM, :] = state
        out[i, HEAD_DIM : HEAD_DIM + 8, :] = addends


def carried_on(got, here, state):
    before, shrunk = jnp.zeros_like(state), jnp.zeros((1, HEAD_DIM), jnp.float32)
    passed = jnp.ones((1, HEAD_DIM), jnp.float32)
    for j in range(8):
        mine = (here == j).astype(jnp.float32)
        decay = jnp.sum(got[j, HEAD_DIM : HEAD_DIM + 8, :].astype(jnp.float32), 0, keepdims=True)
        before = before + mine * state
        shrunk = shrunk + mine * passed
        state = decay * state + got[j, 0:HEAD_DIM, :].astype(jnp.float32)
        passed = passed * decay
    return before, shrunk, state, passed


def project_kernel(place, rates, *refs):
    xs = refs[:8]
    w_ref, cos_ref, sin_ref, q_hbm, k_hbm, v_hbm, p_hbm, o_hbm, s_out = refs[8:17]
    x_buf, q_out, k_out, v_out, p_out, sems = refs[17:]
    core = place[1]

    cut = 3 * HEAD_DIM
    copies = []
    for j in range(8):
        copies.append(pltpu.make_async_copy(xs[j], x_buf.at[pl.ds(j * BLOCK, BLOCK)], sems.at[j]))
        copies[-1].start()

    def start_row(j):
        here = lax.rem(place[0] - j % 4 + 4, 4)
        mine = core if j < 4 else 1 - core
        return pl.multiple_of((here * 2 + mine) * BLOCK, BLOCK)

    def project(block_of):
        half = 2
        for g in range(8 // half):
            for j in range(half):
                copies[g * half + j].wait()
            weights = jnp.concatenate(
                [block_of(a, b) for a in range(8) for b in range(8)], axis=0
            )
            raw = jnp.dot(
                x_buf[pl.ds(g * half * BLOCK, half * BLOCK), :],
                weights,
                preferred_element_type=jnp.float32,
            )
            for j in range(half):
                at = start_row(g * half + j)
                rows = pl.ds(at, BLOCK)
                cosine = cos_ref[rows, :]
                sine = sin_ref[rows, :]
                part = raw[j * BLOCK : (j + 1) * BLOCK, :]
                q = part[:, :HEAD_DIM]
                k = part[:, HEAD_DIM : 2 * HEAD_DIM]
                v = part[:, 2 * HEAD_DIM :]
                q = q * cosine + pltpu.roll(q, HEAD_DIM // 2, 1) * sine
                k = k * cosine + pltpu.roll(k, HEAD_DIM // 2, 1) * sine
                q_out[rows, :] = q.astype(jnp.bfloat16)
                k_out[rows, :] = k.astype(jnp.bfloat16)
                v_out[rows, :] = v.astype(jnp.bfloat16)

    @pl.when(core == 0)
    def _():
        for a in range(8):
            pltpu.make_async_copy(
                w_ref.at[a, :, :, pl.ds(cut, HEAD_DIM)], o_hbm.at[a], sems.at[9]
            ).start()
        project(lambda a, b: w_ref[a, b, :, :cut])

    @pl.when(core == 1)
    def _():
        for a in range(8):
            pltpu.make_async_copy(
                w_ref.at[:, a, :, pl.ds(cut, HEAD_DIM)], o_hbm.at[a], sems.at[9]
            ).start()
        project(lambda a, b: w_ref[b, a, :, :cut])

    leaving = [pltpu.make_async_copy(w_ref.at[:, :, :, pl.ds(cut, HEAD_DIM)], o_hbm, sems.at[9])]
    for j, (kept, out) in enumerate(((q_out, q_hbm), (k_out, k_hbm), (v_out, v_hbm))):
        leaving.append(pltpu.make_async_copy(kept, out, sems.at[j]))
        leaving[-1].start()

    row = lax.broadcasted_iota(jnp.int32, (BLOCK, BLOCK), 0).astype(jnp.float32)
    scale = HEAD_DIM**-0.5
    state = jnp.zeros((HEAD_DIM, HEAD_DIM), jnp.float32)
    total = jnp.float32(0.0)
    for b in range(8):
        rate = rates[b, 0]
        total = total + rate
        rows = pl.ds(b * BLOCK, BLOCK)
        p_out[b] = state.astype(jnp.bfloat16)
        tail = jnp.exp(-(BLOCK - 1.0 - row) * rate) * scale
        fed = (k_out[rows, :].astype(jnp.float32) * tail).astype(jnp.bfloat16)
        kv = lax.dot_general(
            fed, v_out[rows, :], (((0,), (0,)), ((), ())), preferred_element_type=jnp.float32
        )
        state = jnp.exp(jnp.full((HEAD_DIM, HEAD_DIM), -float(BLOCK), jnp.float32) * rate) * state + kv
    leaving.append(pltpu.make_async_copy(p_out, p_hbm, sems.at[3]))
    leaving[-1].start()
    write_message(s_out, state, jnp.exp(jnp.full((8, HEAD_DIM), -float(BLOCK), jnp.float32) * total))
    for copy in leaving:
        copy.wait()


def projected(place, rates, chunks, weights, cosine, sine):
    span = 8 * BLOCK
    rows = pltpu.HBM((span, HEAD_DIM), jnp.bfloat16)
    return pl.pallas_call(
        project_kernel,
        out_shape=(
            rows,
            rows,
            rows,
            pltpu.HBM((8, HEAD_DIM, HEAD_DIM), jnp.bfloat16),
            pltpu.HBM((8, 8, 32, HEAD_DIM), jnp.bfloat16),
            jax.ShapeDtypeStruct(MESSAGES, jnp.bfloat16),
        ),
        in_specs=[SMEM, SMEM] + [ANY] * 8 + [VMEM] * 3,
        out_specs=(HBM,) * 5 + (VMEM,),
        scratch_shapes=[
            pltpu.VMEM((span, 2048), jnp.bfloat16),
            pltpu.VMEM((span, HEAD_DIM), jnp.bfloat16),
            pltpu.VMEM((span, HEAD_DIM), jnp.bfloat16),
            pltpu.VMEM((span, HEAD_DIM), jnp.bfloat16),
            pltpu.VMEM((8, HEAD_DIM, HEAD_DIM), jnp.bfloat16),
            pltpu.SemaphoreType.DMA((10,)),
        ],
        compiler_params=pltpu.CompilerParams(vmem_limit_bytes=24 << 20),
        cost_estimate=pl.CostEstimate(
            flops=1700000000, bytes_accessed=7 << 20, transcendentals=1 << 18
        ),
    )(place, rates, *chunks, weights, cosine, sine)


def local_kernel(rates, q_hbm, k_hbm, v_hbm, p_hbm, l_hbm, q_ref, k_ref, v_ref, p_ref, l_out, sems):
    pairs = ((q_hbm, q_ref), (k_hbm, k_ref), (v_hbm, v_ref), (p_hbm, p_ref))
    copies = [pltpu.make_async_copy(a, b, sems.at[j]) for j, (a, b) in enumerate(pairs)]
    for copy in copies:
        copy.start()
    for copy in copies:
        copy.wait()
    row = lax.broadcasted_iota(jnp.int32, (BLOCK, BLOCK), 0).astype(jnp.float32)
    col = lax.broadcasted_iota(jnp.int32, (BLOCK, BLOCK), 1).astype(jnp.float32)
    gap = row - col
    scale = HEAD_DIM**-0.5
    for b in range(8):
        rate = rates[b, 0]
        rows = pl.ds(b * BLOCK, BLOCK)
        q, k, v = q_ref[rows, :], k_ref[rows, :], v_ref[rows, :]
        inside = jnp.where(gap >= 0.0, jnp.exp(-jnp.maximum(gap, 0.0) * rate) * scale, 0.0)
        scores = lax.dot_general(q, k, (((1,), (1,)), ((), ())), preferred_element_type=jnp.float32)
        out = jnp.dot(
            (scores * inside).astype(jnp.bfloat16), v, preferred_element_type=jnp.float32
        )
        if b > 0:
            cross = jnp.dot(q, p_ref[b], preferred_element_type=jnp.float32)
            out = out + cross * jnp.exp(-(row + 1.0) * rate)
        l_out[rows, :] = out
    leaving = pltpu.make_async_copy(l_out, l_hbm, sems.at[4])
    leaving.start()
    leaving.wait()


def local_part(rates, q, k, v, before):
    return pl.pallas_call(
        local_kernel,
        out_shape=pltpu.HBM(q.shape, jnp.float32),
        in_specs=[SMEM] + [ANY] * 4,
        out_specs=HBM,
        scratch_shapes=[
            pltpu.VMEM(q.shape, jnp.bfloat16),
            pltpu.VMEM(q.shape, jnp.bfloat16),
            pltpu.VMEM(q.shape, jnp.bfloat16),
            pltpu.VMEM(before.shape, jnp.bfloat16),
            pltpu.VMEM(q.shape, jnp.float32),
            pltpu.SemaphoreType.DMA((5,)),
        ],
        compiler_params=pltpu.CompilerParams(vmem_limit_bytes=4 << 20),
        cost_estimate=pl.CostEstimate(
            flops=1000000000, bytes_accessed=2 << 20, transcendentals=1 << 18
        ),
    )(rates, q, k, v, before)


def row_kernel(place, got, out, before_out, shrunk_out):
    zero = jnp.zeros((HEAD_DIM, HEAD_DIM), jnp.float32)
    before, shrunk, end, passed = carried_on(got, place[3], zero)
    write_message(out, end, jnp.broadcast_to(passed, (8, HEAD_DIM)))
    before_out[...] = before
    shrunk_out[...] = jnp.broadcast_to(shrunk, (8, HEAD_DIM))


def along_row(place, got):
    return pl.pallas_call(
        row_kernel,
        out_shape=(
            jax.ShapeDtypeStruct(MESSAGES, jnp.bfloat16),
            jax.ShapeDtypeStruct((HEAD_DIM, HEAD_DIM), jnp.float32),
            jax.ShapeDtypeStruct((8, HEAD_DIM), jnp.float32),
        ),
        in_specs=[SMEM, VMEM],
        out_specs=(VMEM,) * 3,
        compiler_params=pltpu.CompilerParams(vmem_limit_bytes=2 << 20),
        cost_estimate=pl.CostEstimate(flops=1000000, bytes_accessed=1 << 18, transcendentals=0),
    )(place, got)


def hidden_kernel(place, rates, got, before_ref, shrunk_ref, gain_ref, init_hbm, q_hbm, l_hbm, out_ref, *rest):
    q_ref, l_ref, init_ref, sems = rest
    pairs = ((init_hbm, init_ref), (q_hbm, q_ref), (l_hbm, l_ref))
    copies = [pltpu.make_async_copy(a, b, sems.at[j]) for j, (a, b) in enumerate(pairs)]
    for copy in copies:
        copy.start()
    copies[0].wait()
    start = carried_on(got, place[2], init_ref[...])[0]
    row = lax.broadcasted_iota(jnp.int32, (BLOCK, HEAD_DIM), 0).astype(jnp.float32)
    copies[1].wait()
    copies[2].wait()
    state = (before_ref[...] + shrunk_ref[0:1, :] * start).astype(jnp.bfloat16)
    gain = gain_ref[...]
    before = jnp.float32(0.0)
    for b in range(8):
        rate = rates[b, 0]
        rows = pl.ds(b * BLOCK, BLOCK)
        carried = jnp.dot(q_ref[rows, :], state, preferred_element_type=jnp.float32)
        mixed = l_ref[rows, :] + carried * jnp.exp(-(row + 1.0) * rate - BLOCK * before)
        norm = lax.rsqrt(jnp.mean(mixed * mixed, axis=-1, keepdims=True) + EPS)
        out_ref[b] = (mixed * norm * gain).astype(jnp.bfloat16)
        before = before + rate


def hidden_part(*args):
    return pl.pallas_call(
        hidden_kernel,
        out_shape=jax.ShapeDtypeStruct((8, BLOCK, HEAD_DIM), jnp.bfloat16),
        in_specs=[SMEM, SMEM] + [VMEM] * 4 + [ANY] * 3,
        out_specs=VMEM,
        scratch_shapes=[
            pltpu.VMEM((8 * BLOCK, HEAD_DIM), jnp.bfloat16),
            pltpu.VMEM((8 * BLOCK, HEAD_DIM), jnp.float32),
            pltpu.VMEM((HEAD_DIM, HEAD_DIM), jnp.float32),
            pltpu.SemaphoreType.DMA((3,)),
        ],
        compiler_params=pltpu.CompilerParams(vmem_limit_bytes=4 << 20),
        cost_estimate=pl.CostEstimate(
            flops=40000000, bytes_accessed=1 << 20, transcendentals=1 << 17
        ),
    )(*args)


def out_kernel(place, h_ref, same_ref, other_hbm, out_ref, other_buf, sems):
    copies = []
    for j in range(4):
        copies.append(pltpu.make_async_copy(other_hbm.at[j], other_buf.at[j], sems.at[j]))
        copies[-1].start()
    total = None
    for j in range(8):
        here = lax.rem(place[0] - j % 4 + 4, 4)
        core = place[1] if j < 4 else 1 - place[1]
        if j >= 4:
            copies[j - 4].wait()
        part = lax.dot_general(
            h_ref[here * 2 + core],
            same_ref[j] if j < 4 else other_buf[j - 4],
            (((1,), (1,)), ((), ())),
            preferred_element_type=jnp.float32,
        )
        total = part if total is None else total + part
    out_ref[...] = total.astype(jnp.bfloat16)


def out_part(place, hidden, same, other):
    return pl.pallas_call(
        out_kernel,
        out_shape=jax.ShapeDtypeStruct((BLOCK, 2048), jnp.bfloat16),
        in_specs=[SMEM, VMEM, VMEM, ANY],
        out_specs=VMEM,
        scratch_shapes=[
            pltpu.VMEM((4, 2048, HEAD_DIM), jnp.bfloat16),
            pltpu.SemaphoreType.DMA((4,)),
        ],
        compiler_params=pltpu.CompilerParams(vmem_limit_bytes=24 << 20),
        cost_estimate=pl.CostEstimate(
            flops=540000000, bytes_accessed=5 << 20, transcendentals=0
        ),
    )(place, hidden, same, other)


def rotation_tables(first, rows):
    half = HEAD_DIM // 2
    inv_freq = ROPE_BASE ** (-jnp.arange(half, dtype=jnp.float32) / half)
    positions = (first + jnp.arange(rows, dtype=jnp.int32)).astype(jnp.float32)
    angles = positions[:, None] * inv_freq[None, :]
    cosine, sine = jnp.cos(angles), jnp.sin(angles)
    return (
        jnp.concatenate([cosine, cosine], axis=-1),
        jnp.concatenate([-sine, sine], axis=-1),
    )


def shards(tokens, norm_gain, w_query, w_key, w_value, decay_rate, state_init, out_gain, w_out):
    where = lax.axis_index(SP)
    place = jnp.stack([lax.axis_index(a) for a in ("tp_0", "tp_1", "sp_0", "sp_1")]).astype(jnp.int32)
    normed = normalized(tokens, norm_gain)
    packed = jnp.concatenate([w_query, w_key, w_value, w_out.T], axis=1)[None]
    lined = along(jnp.broadcast_to(packed, (8, 32, 4 * HEAD_DIM)), True)
    tables = rotation_tables(where * (8 * BLOCK), 8 * BLOCK)
    chunks, cosine, sine = token_chunks(normed, tables)
    lined = lined.reshape(1, 256, 4 * HEAD_DIM)
    weights = along(jnp.broadcast_to(lined, (8, 256, 4 * HEAD_DIM)), False)
    weights = weights.reshape(8, 8, 32, 4 * HEAD_DIM)
    q, k, v, before, own_out, sliced = projected(place, decay_rate, chunks, weights, cosine, sine)
    out_chunks = late_chunks(own_out.reshape(2048, HEAD_DIM))
    local_out = local_part(decay_rate, in_hbm(q), in_hbm(k), in_hbm(v), in_hbm(before))
    got = lax.all_to_all(sliced, "sp_1", 0, 0, tiled=True)
    row_end, row_before, shrunk = along_row(place, got)
    got = lax.all_to_all(row_end, "sp_0", 0, 0, tiled=True)
    hidden = hidden_part(
        place,
        decay_rate,
        got,
        row_before,
        shrunk,
        out_gain[None],
        in_hbm(state_init[0]),
        in_hbm(q),
        in_hbm(local_out),
    )
    mine = lax.all_to_all(hidden, TP, 0, 0, tiled=True)
    return out_part(place, mine, *out_chunks)


def solution(mesh):
    split = Mesh(mesh.devices.reshape(8, 8, 4, 2), SP + TP)
    in_specs = (
        P(SP + TP, None),
        P(),
        P(SP, TP),
        P(SP, TP),
        P(SP, TP),
        P(SP, TP),
        P(TP, None, None),
        P(TP),
        P(TP, SP),
    )
    return jax.shard_map(
        shards, mesh=split, in_specs=in_specs, out_specs=P(SP + TP, None), check_vma=False
    )
```

profile of v0, /device:TPU:1, one launch (start us, length us, event | category | flops | bytes accessed | tf_op | source)
XLA Modules:
  0.0 168.4 jit_solution(6046534495765615979)
XLA Ops:
  0.8 20.0 %all_to_all.25 = bf16[8,32,512]{2,1,0:T(8,128)(2,1)S(1)} all-to-all(bf16[8,32,512]{2,1,0:T(8,128)(2,1)S(1)} %broadcast_in_dim.22), channel_id=1, replica_groups={{0,8,16,24,32,40,48,56},{2,10,18,26,34,42,50,58},{4,12,20,28,36,44,52,6..., dimensions={0} | all-to-all | bytes 524288 | tf_op jit(solution)/shard_map/all_to_all | solution.py:40
  20.8 1.5 broadcast_in_dim.24
  22.3 6.8 %all-to-all-start.1 = ((bf16[8,256,512]{2,1,0:T(8,128)(2,1)}), bf16[8,256,512]{2,1,0:T(8,128)(2,1)S(1)}, u32[]{:S(2)}, u32[]{:S(2)}) async-start(bf16[8,256,512]{2,1,0:T(8,128)(2,1)} %broadcast_in_dim.24), calls=%async_computation.1 | async-start | bytes 4194304 | tf_op jit(solution)/shard_map/all_to_all | solution.py:40
  29.1 2.1 %shard_map.91.refs_0_ = bf16[128,2048]{1,0:T(8,128)(2,1)} custom-call(bf16[128,2048]{1,0:T(8,128)(2,1)} %x_hbm.1, f32[1,2048]{1,0:T(1,128)} %bitcast.19), custom_call_target="tpu_custom_call" | custom-call | flops 2000000 | bytes 1048576 | tf_op jit(solution)/shard_map/pallas_call | solution.py:100
  31.2 4.3 %collective-permute-start.3 = (bf16[128,2048]{1,0:T(8,128)(2,1)}, bf16[128,2048]{1,0:T(8,128)(2,1)}, u32[]{:S(2)}, u32[]{:S(2)}) collective-permute-start(bf16[128,2048]{1,0:T(8,128)(2,1)} %shard_map.91.refs_0_), channel_id=1, source_target_pairs={{0,1},{1,0},{2,3},{3,2},{4,5},{5,4},{6,7},{7,6},{8,9},{9,8},{10,11... | collective-permute-start | bytes 1572872 | tf_op jit(solution)/shard_map/ppermute | solution.py:49
  35.5 4.4 %collective-permute-start.2 = (bf16[128,2048]{1,0:T(8,128)(2,1)}, bf16[128,2048]{1,0:T(8,128)(2,1)}, u32[]{:S(2)}, u32[]{:S(2)}) collective-permute-start(bf16[128,2048]{1,0:T(8,128)(2,1)} %shard_map.91.refs_0_), channel_id=1, source_target_pairs={{0,6},{2,0},{4,2},{6,4},{1,7},{3,1},{5,3},{7,5},{8,14},{10,8},{12,... | collective-permute-start | bytes 1572872 | tf_op jit(solution)/shard_map/ppermute | solution.py:45
  39.9 2.4 %collective-permute-start.1 = (bf16[128,2048]{1,0:T(8,128)(2,1)}, bf16[128,2048]{1,0:T(8,128)(2,1)}, u32[]{:S(2)}, u32[]{:S(2)}) collective-permute-start(bf16[128,2048]{1,0:T(8,128)(2,1)} %shard_map.91.refs_0_), channel_id=1, source_target_pairs={{0,4},{2,6},{4,0},{6,2},{1,5},{3,7},{5,1},{7,3},{8,12},{10,14},{12... | collective-permute-start | bytes 1572872 | tf_op jit(solution)/shard_map/ppermute | solution.py:45
  42.3 2.5 %collective-permute-start = (bf16[128,2048]{1,0:T(8,128)(2,1)}, bf16[128,2048]{1,0:T(8,128)(2,1)}, u32[]{:S(2)}, u32[]{:S(2)}) collective-permute-start(bf16[128,2048]{1,0:T(8,128)(2,1)} %shard_map.91.refs_0_), channel_id=1, source_target_pairs={{0,2},{2,4},{4,6},{6,0},{1,3},{3,5},{5,7},{7,1},{8,10},{10,12},{12... | collective-permute-start | bytes 1572872 | tf_op jit(solution)/shard_map/ppermute | solution.py:45
  44.9 1.9 %fusion = (f32[1024,64]{1,0:T(8,128)S(1)}, f32[1024,64]{1,0:T(8,128)S(1)}, f32[1024,64]{1,0:T(8,128)S(1)}) fusion(f32[64]{0:T(128)S(1)} %multiply_power_fusion, f32[1024]{0:T(1024)S(1)} %add_convert_fusion), kind=kLoop, calls=%fused_computation.4 | loop fusion | flops 131072 | bytes 790784 | tf_op jit(solution)/shard_map/neg | solution.py:421
  47.1 9.7 %collective-permute-done.1.refs_2_ = bf16[128,2048]{1,0:T(8,128)(2,1)} collective-permute-done((bf16[128,2048]{1,0:T(8,128)(2,1)}, bf16[128,2048]{1,0:T(8,128)(2,1)}, u32[]{:S(2)}, u32[]{:S(2)}) %collective-permute-start.1) | collective-permute-done | bytes 524320 | tf_op jit(solution)/shard_map/ppermute | solution.py:45
  56.8 5.7 %collective-permute-done.2.refs_3_ = bf16[128,2048]{1,0:T(8,128)(2,1)} collective-permute-done((bf16[128,2048]{1,0:T(8,128)(2,1)}, bf16[128,2048]{1,0:T(8,128)(2,1)}, u32[]{:S(2)}, u32[]{:S(2)}) %collective-permute-start.2) | collective-permute-done | bytes 524320 | tf_op jit(solution)/shard_map/ppermute | solution.py:45
  62.5 2.9 %collective-permute-start.6 = (bf16[128,2048]{1,0:T(8,128)(2,1)}, bf16[128,2048]{1,0:T(8,128)(2,1)}, u32[]{:S(2)}, u32[]{:S(2)}) collective-permute-start(bf16[128,2048]{1,0:T(8,128)(2,1)} %collective-permute-done.2.refs_3_), channel_id=1, source_target_pairs={{0,1},{1,0},{2,3},{3,2},{4,5},{5,4},{6,7},{7,6},{8,9},{9,8},{10,11... | collective-permute-start | bytes 1572872 | tf_op jit(solution)/shard_map/ppermute | solution.py:49
  65.5 3.2 %collective-permute-done.refs_1_ = bf16[128,2048]{1,0:T(8,128)(2,1)} collective-permute-done((bf16[128,2048]{1,0:T(8,128)(2,1)}, bf16[128,2048]{1,0:T(8,128)(2,1)}, u32[]{:S(2)}, u32[]{:S(2)}) %collective-permute-start) | collective-permute-done | bytes 524320 | tf_op jit(solution)/shard_map/ppermute | solution.py:45
  68.7 2.4 %collective-permute-start.4 = (bf16[128,2048]{1,0:T(8,128)(2,1)}, bf16[128,2048]{1,0:T(8,128)(2,1)}, u32[]{:S(2)}, u32[]{:S(2)}) collective-permute-start(bf16[128,2048]{1,0:T(8,128)(2,1)} %collective-permute-done.refs_1_), channel_id=1, source_target_pairs={{0,1},{1,0},{2,3},{3,2},{4,5},{5,4},{6,7},{7,6},{8,9},{9,8},{10,11... | collective-permute-start | bytes 1572872 | tf_op jit(solution)/shard_map/ppermute | solution.py:49
  71.1 1.9 %collective-permute-start.5 = (bf16[128,2048]{1,0:T(8,128)(2,1)}, bf16[128,2048]{1,0:T(8,128)(2,1)}, u32[]{:S(2)}, u32[]{:S(2)}) collective-permute-start(bf16[128,2048]{1,0:T(8,128)(2,1)} %collective-permute-done.1.refs_2_), channel_id=1, source_target_pairs={{0,1},{1,0},{2,3},{3,2},{4,5},{5,4},{6,7},{7,6},{8,9},{9,8},{10,11... | collective-permute-start | bytes 1572872 | tf_op jit(solution)/shard_map/ppermute | solution.py:49
  73.2 2.0 %collective-permute-done.5.refs_6_ = bf16[128,2048]{1,0:T(8,128)(2,1)} collective-permute-done((bf16[128,2048]{1,0:T(8,128)(2,1)}, bf16[128,2048]{1,0:T(8,128)(2,1)}, u32[]{:S(2)}, u32[]{:S(2)}) %collective-permute-start.5) | collective-permute-done | bytes 524320 | tf_op jit(solution)/shard_map/ppermute | solution.py:49
  75.2 6.3 %shard_map.92 = (bf16[1024,128]{1,0:T(8,128)(2,1)}, bf16[1024,128]{1,0:T(8,128)(2,1)}, bf16[1024,128]{1,0:T(8,128)(2,1)}, bf16[8,128,128]{2,1,0:T(8,128)(2,1)}, ...) custom-call(s32[4]{0:T(128)S(1)} %pad_add_fusion.place, f32[8,1]{1,0:T(8,128)S(1)} %copy.12.rates, ...), custom_call_target="tpu_custom_call" | custom-call | flops 1700000000 | bytes 7340032 | tf_op jit(solution)/shard_map/pallas_call | solution.py:232
  81.5 2.2 %collective-permute-start.9 = (bf16[2048,128]{1,0:T(8,128)(2,1)}, bf16[2048,128]{1,0:T(8,128)(2,1)S(1)}, u32[]{:S(2)}, u32[]{:S(2)}) collective-permute-start(bf16[2048,128]{1,0:T(8,128)(2,1)} %bitcast.14), channel_id=1, source_target_pairs={{0,6},{2,0},{4,2},{6,4},{1,7},{3,1},{5,3},{7,5},{8,14},{10,8},{12,... | collective-permute-start | bytes 1572872 | tf_op jit(solution)/shard_map/ppermute | solution.py:45
  83.7 2.4 %collective-permute-start.8 = (bf16[2048,128]{1,0:T(8,128)(2,1)}, bf16[2048,128]{1,0:T(8,128)(2,1)S(1)}, u32[]{:S(2)}, u32[]{:S(2)}) collective-permute-start(bf16[2048,128]{1,0:T(8,128)(2,1)} %bitcast.15), channel_id=1, source_target_pairs={{0,4},{2,6},{4,0},{6,2},{1,5},{3,7},{5,1},{7,3},{8,12},{10,14},{12... | collective-permute-start | bytes 1572872 | tf_op jit(solution)/shard_map/ppermute | solution.py:45
  86.2 2.5 %collective-permute-start.7 = (bf16[2048,128]{1,0:T(8,128)(2,1)}, bf16[2048,128]{1,0:T(8,128)(2,1)S(1)}, u32[]{:S(2)}, u32[]{:S(2)}) collective-permute-start(bf16[2048,128]{1,0:T(8,128)(2,1)} %bitcast.16), channel_id=1, source_target_pairs={{0,2},{2,4},{4,6},{6,0},{1,3},{3,5},{5,7},{7,1},{8,10},{10,12},{12... | collective-permute-start | bytes 1572872 | tf_op jit(solution)/shard_map/ppermute | solution.py:45
  88.7 8.2 %collective-permute-done.9.refs_3_ = bf16[2048,128]{1,0:T(8,128)(2,1)S(1)} collective-permute-done((bf16[2048,128]{1,0:T(8,128)(2,1)}, bf16[2048,128]{1,0:T(8,128)(2,1)S(1)}, u32[]{:S(2)}, u32[]{:S(2)}) %collective-permute-start.9) | collective-permute-done | bytes 524320 | tf_op jit(solution)/shard_map/ppermute | solution.py:45
  97.0 3.5 %collective-permute-done.8.refs_2_ = bf16[2048,128]{1,0:T(8,128)(2,1)S(1)} collective-permute-done((bf16[2048,128]{1,0:T(8,128)(2,1)}, bf16[2048,128]{1,0:T(8,128)(2,1)S(1)}, u32[]{:S(2)}, u32[]{:S(2)}) %collective-permute-start.8) | collective-permute-done | bytes 524320 | tf_op jit(solution)/shard_map/ppermute | solution.py:45
  100.5 12.0 %collective-permute-done.7.refs_1_ = bf16[2048,128]{1,0:T(8,128)(2,1)S(1)} collective-permute-done((bf16[2048,128]{1,0:T(8,128)(2,1)}, bf16[2048,128]{1,0:T(8,128)(2,1)S(1)}, u32[]{:S(2)}, u32[]{:S(2)}) %collective-permute-start.7) | collective-permute-done | bytes 524320 | tf_op jit(solution)/shard_map/ppermute | solution.py:45
  113.2 1.5 shard_map.96.same_ref
  114.8 2.4 %collective-permute-start.10 = (bf16[4,2048,128]{2,1,0:T(8,128)(2,1)S(1)}, bf16[4,2048,128]{2,1,0:T(8,128)(2,1)}, u32[]{:S(2)}, u32[]{:S(2)}) collective-permute-start(bf16[4,2048,128]{2,1,0:T(8,128)(2,1)S(1)} %shard_map.96.same_ref), channel_id=1, source_target_pairs={{0,1},{1,0},{2,3},{3,2},{4,5},{5,4},{6,7},{7,6},{8,9},{9,8},{10,11... | collective-permute-start | bytes 6291464 | tf_op jit(solution)/shard_map/ppermute | solution.py:49
  117.2 16.7 %all_to_all.26.got = bf16[8,136,128]{2,1,0:T(8,128)(2,1)S(1)} all-to-all(bf16[8,136,128]{2,1,0:T(8,128)(2,1)S(1)} %get-tuple-element.20), channel_id=1, replica_groups=mesh['sp_0'=8,'sp_1'=8,'tp_0'=4,'tp_1'=2] {'sp_1'}, dimensions={0} | all-to-all | bytes 557056 | tf_op jit(solution)/shard_map/all_to_all | solution.py:439
  135.2 5.4 %all-to-all-start.3 = ((bf16[8,136,128]{2,1,0:T(8,128)(2,1)}), bf16[8,136,128]{2,1,0:T(8,128)(2,1)S(1)}, u32[]{:S(2)}, u32[]{:S(2)}) async-start(bf16[8,136,128]{2,1,0:T(8,128)(2,1)} %get-tuple-element.21), calls=%async_computation.3 | async-start | bytes 557056 | tf_op jit(solution)/shard_map/all_to_all | solution.py:441
  140.6 3.3 %shard_map.94.l_hbm = f32[1024,128]{1,0:T(8,128)} custom-call(f32[8,1]{1,0:T(8,128)S(1)} %copy.12.rates, bf16[1024,128]{1,0:T(8,128)(2,1)} %get-tuple-element.24.q_hbm, bf16[1024,128]{1,0:T(8,128)(2,1)} %get-tuple-element.25.k_hbm, bf16[1024,128]{1,0:T(8,128)(2,1)} %get-tuple-element.26.v_hbm, bf16[8,128,128]{2,1,0:T(8,128)(2,1)} %get-tuple-element.27.p_hbm), custom_call_target="tpu_custom_call" | custom-call | flops 1000000000 | bytes 2097152 | tf_op jit(solution)/shard_map/pallas_call | solution.py:289
  143.9 7.7 %all-to-all-done.3.got = bf16[8,136,128]{2,1,0:T(8,128)(2,1)S(1)} async-done(((bf16[8,136,128]{2,1,0:T(8,128)(2,1)}), bf16[8,136,128]{2,1,0:T(8,128)(2,1)S(1)}, u32[]{:S(2)}, u32[]{:S(2)}) %all-to-all-start.3) | async-done | bytes 278560 | tf_op jit(solution)/shard_map/all_to_all | solution.py:441
  151.6 2.2 %shard_map.95 = bf16[8,128,128]{2,1,0:T(8,128)(2,1)S(1)} custom-call(s32[4]{0:T(128)S(1)} %pad_add_fusion.place, f32[8,1]{1,0:T(8,128)S(1)} %copy.12.rates, bf16[8,136,128]{2,1,0:T(8,128)(2,1)S(1)} %all-to-all-done.3.got, f32[128,128]{1,0:T(8,128)S(1)} %get-tuple-element.22.before_ref, f32[8,128]{1,0:T(8,128)S(1)} %get-tuple-element.23.shrunk_ref, ...), custom_call_target="tpu_custom_call" | custom-call | flops 40000000 | bytes 1048576 | tf_op jit(solution)/shard_map/pallas_call | solution.py:357
  153.8 11.0 %all_to_all.27.h_ref = bf16[8,128,128]{2,1,0:T(8,128)(2,1)S(1)} all-to-all(bf16[8,128,128]{2,1,0:T(8,128)(2,1)S(1)} %shard_map.95), channel_id=1, replica_groups=mesh['sp_0'=8,'sp_1'=8,'tp_0'=4,'tp_1'=2] {'tp_0','tp_1'}, dimensions={0} | all-to-all | bytes 524288 | tf_op jit(solution)/shard_map/all_to_all | solution.py:453
  164.8 3.6 %shard_map.97 = bf16[128,2048]{1,0:T(8,128)(2,1)} custom-call(s32[4]{0:T(128)S(1)} %pad_add_fusion.place, bf16[8,128,128]{2,1,0:T(8,128)(2,1)S(1)} %all_to_all.27.h_ref, bf16[4,2048,128]{2,1,0:T(8,128)(2,1)S(1)} %shard_map.96.same_ref, bf16[4,2048,128]{2,1,0:T(8,128)(2,1)} %collective-permute-done.10.other_hbm), custom_call_target="tpu_custom_call" | custom-call | flops 540000000 | bytes 5242880 | tf_op jit(solution)/shard_map/pallas_call | solution.py:397
  (23 shorter events, 3.4 us)
Async XLA Ops:
  22.3 52.9 %all-to-all-start.1 = ((bf16[8,256,512]{2,1,0:T(8,128)(2,1)}), bf16[8,256,512]{2,1,0:T(8,128)(2,1)S(1)}, u32[]{:S(2)}, u32[]{:S(2)}) async-start(bf16[8,256,512]{2,1,0:T(8,128)(2,1)} %broadcast_in_dim.24), calls=%async_computation.1 | async-start | bytes 4194304 | tf_op jit(solution)/shard_map/all_to_all | solution.py:40
  31.2 42.0 %collective-permute-start.3 = (bf16[128,2048]{1,0:T(8,128)(2,1)}, bf16[128,2048]{1,0:T(8,128)(2,1)}, u32[]{:S(2)}, u32[]{:S(2)}) collective-permute-start(bf16[128,2048]{1,0:T(8,128)(2,1)} %shard_map.91.refs_0_), channel_id=1, source_target_pairs={{0,1},{1,0},{2,3},{3,2},{4,5},{5,4},{6,7},{7,6},{8,9},{9,8},{10,11... | collective-permute-start | bytes 1572872 | tf_op jit(solution)/shard_map/ppermute | solution.py:49
  35.5 27.0 %collective-permute-start.2 = (bf16[128,2048]{1,0:T(8,128)(2,1)}, bf16[128,2048]{1,0:T(8,128)(2,1)}, u32[]{:S(2)}, u32[]{:S(2)}) collective-permute-start(bf16[128,2048]{1,0:T(8,128)(2,1)} %shard_map.91.refs_0_), channel_id=1, source_target_pairs={{0,6},{2,0},{4,2},{6,4},{1,7},{3,1},{5,3},{7,5},{8,14},{10,8},{12,... | collective-permute-start | bytes 1572872 | tf_op jit(solution)/shard_map/ppermute | solution.py:45
  39.9 16.9 %collective-permute-start.1 = (bf16[128,2048]{1,0:T(8,128)(2,1)}, bf16[128,2048]{1,0:T(8,128)(2,1)}, u32[]{:S(2)}, u32[]{:S(2)}) collective-permute-start(bf16[128,2048]{1,0:T(8,128)(2,1)} %shard_map.91.refs_0_), channel_id=1, source_target_pairs={{0,4},{2,6},{4,0},{6,2},{1,5},{3,7},{5,1},{7,3},{8,12},{10,14},{12... | collective-permute-start | bytes 1572872 | tf_op jit(solution)/shard_map/ppermute | solution.py:45
  42.3 26.4 %collective-permute-start = (bf16[128,2048]{1,0:T(8,128)(2,1)}, bf16[128,2048]{1,0:T(8,128)(2,1)}, u32[]{:S(2)}, u32[]{:S(2)}) collective-permute-start(bf16[128,2048]{1,0:T(8,128)(2,1)} %shard_map.91.refs_0_), channel_id=1, source_target_pairs={{0,2},{2,4},{4,6},{6,0},{1,3},{3,5},{5,7},{7,1},{8,10},{10,12},{12... | collective-permute-start | bytes 1572872 | tf_op jit(solution)/shard_map/ppermute | solution.py:45
  44.9 28.1 %copy-start.4 = (f32[8,1]{0,1:T(1,128)S(1)}, f32[8,1]{0,1:T(1,128)}, u32[]{:S(2)}) copy-start(f32[8,1]{0,1:T(1,128)} %param.14) | copy-start | bytes 100
  62.5 10.7 %collective-permute-start.6 = (bf16[128,2048]{1,0:T(8,128)(2,1)}, bf16[128,2048]{1,0:T(8,128)(2,1)}, u32[]{:S(2)}, u32[]{:S(2)}) collective-permute-start(bf16[128,2048]{1,0:T(8,128)(2,1)} %collective-permute-done.2.refs_3_), channel_id=1, source_target_pairs={{0,1},{1,0},{2,3},{3,2},{4,5},{5,4},{6,7},{7,6},{8,9},{9,8},{10,11... | collective-permute-start | bytes 1572872 | tf_op jit(solution)/shard_map/ppermute | solution.py:49
  68.7 4.5 %collective-permute-start.4 = (bf16[128,2048]{1,0:T(8,128)(2,1)}, bf16[128,2048]{1,0:T(8,128)(2,1)}, u32[]{:S(2)}, u32[]{:S(2)}) collective-permute-start(bf16[128,2048]{1,0:T(8,128)(2,1)} %collective-permute-done.refs_1_), channel_id=1, source_target_pairs={{0,1},{1,0},{2,3},{3,2},{4,5},{5,4},{6,7},{7,6},{8,9},{9,8},{10,11... | collective-permute-start | bytes 1572872 | tf_op jit(solution)/shard_map/ppermute | solution.py:49
  71.1 4.1 %collective-permute-start.5 = (bf16[128,2048]{1,0:T(8,128)(2,1)}, bf16[128,2048]{1,0:T(8,128)(2,1)}, u32[]{:S(2)}, u32[]{:S(2)}) collective-permute-start(bf16[128,2048]{1,0:T(8,128)(2,1)} %collective-permute-done.1.refs_2_), channel_id=1, source_target_pairs={{0,1},{1,0},{2,3},{3,2},{4,5},{5,4},{6,7},{7,6},{8,9},{9,8},{10,11... | collective-permute-start | bytes 1572872 | tf_op jit(solution)/shard_map/ppermute | solution.py:49
  81.5 15.4 %collective-permute-start.9 = (bf16[2048,128]{1,0:T(8,128)(2,1)}, bf16[2048,128]{1,0:T(8,128)(2,1)S(1)}, u32[]{:S(2)}, u32[]{:S(2)}) collective-permute-start(bf16[2048,128]{1,0:T(8,128)(2,1)} %bitcast.14), channel_id=1, source_target_pairs={{0,6},{2,0},{4,2},{6,4},{1,7},{3,1},{5,3},{7,5},{8,14},{10,8},{12,... | collective-permute-start | bytes 1572872 | tf_op jit(solution)/shard_map/ppermute | solution.py:45
  83.7 16.7 %collective-permute-start.8 = (bf16[2048,128]{1,0:T(8,128)(2,1)}, bf16[2048,128]{1,0:T(8,128)(2,1)S(1)}, u32[]{:S(2)}, u32[]{:S(2)}) collective-permute-start(bf16[2048,128]{1,0:T(8,128)(2,1)} %bitcast.15), channel_id=1, source_target_pairs={{0,4},{2,6},{4,0},{6,2},{1,5},{3,7},{5,1},{7,3},{8,12},{10,14},{12... | collective-permute-start | bytes 1572872 | tf_op jit(solution)/shard_map/ppermute | solution.py:45
  86.2 26.3 %collective-permute-start.7 = (bf16[2048,128]{1,0:T(8,128)(2,1)}, bf16[2048,128]{1,0:T(8,128)(2,1)S(1)}, u32[]{:S(2)}, u32[]{:S(2)}) collective-permute-start(bf16[2048,128]{1,0:T(8,128)(2,1)} %bitcast.16), channel_id=1, source_target_pairs={{0,2},{2,4},{4,6},{6,0},{1,3},{3,5},{5,7},{7,1},{8,10},{10,12},{12... | collective-permute-start | bytes 1572872 | tf_op jit(solution)/shard_map/ppermute | solution.py:45
  96.9 15.5 %copy-start.1 = (bf16[2048,128]{1,0:T(8,128)(2,1)}, bf16[2048,128]{1,0:T(8,128)(2,1)S(1)}, u32[]{:S(2)}) copy-start(bf16[2048,128]{1,0:T(8,128)(2,1)S(1)} %collective-permute-done.9.refs_3_) | copy-start | bytes 1572868
  100.5 12.0 %copy-start.2 = (bf16[2048,128]{1,0:T(8,128)(2,1)}, bf16[2048,128]{1,0:T(8,128)(2,1)S(1)}, u32[]{:S(2)}) copy-start(bf16[2048,128]{1,0:T(8,128)(2,1)S(1)} %collective-permute-done.8.refs_2_) | copy-start | bytes 1572868
  112.5 0.8 copy-start.3
  114.8 50.0 %collective-permute-start.10 = (bf16[4,2048,128]{2,1,0:T(8,128)(2,1)S(1)}, bf16[4,2048,128]{2,1,0:T(8,128)(2,1)}, u32[]{:S(2)}, u32[]{:S(2)}) collective-permute-start(bf16[4,2048,128]{2,1,0:T(8,128)(2,1)S(1)} %shard_map.96.same_ref), channel_id=1, source_target_pairs={{0,1},{1,0},{2,3},{3,2},{4,5},{5,4},{6,7},{7,6},{8,9},{9,8},{10,11... | collective-permute-start | bytes 6291464 | tf_op jit(solution)/shard_map/ppermute | solution.py:49
  135.2 16.4 %copy-start = (f32[128]{0:T(128)S(1)}, f32[128]{0:T(128)}, u32[]{:S(2)}) copy-start(f32[128]{0:T(128)} %param.16) | copy-start | bytes 1540
  135.2 16.4 %all-to-all-start.3 = ((bf16[8,136,128]{2,1,0:T(8,128)(2,1)}), bf16[8,136,128]{2,1,0:T(8,128)(2,1)S(1)}, u32[]{:S(2)}, u32[]{:S(2)}) async-start(bf16[8,136,128]{2,1,0:T(8,128)(2,1)} %get-tuple-element.21), calls=%async_computation.3 | async-start | bytes 557056 | tf_op jit(solution)/shard_map/all_to_all | solution.py:441
where the time goes:
time: 169 us; the launch traced here: 168 us
  waiting for transfers between devices  52.1 us (31%)
  blocking collectives  47.7 us (28%)
  starting transfers between devices  42.7 us (25%)
  Pallas kernels  20.2 us (12%)
  other arithmetic  3.08 us (2%)
  local copies, waits for them, and re-layouts  2.43 us (1%)
    ppermute x6, waiting for transfers between devices, shifted(): return lax.ppermute(own, 'tp_0', [(i, (i + d) % n) for i in range(n)])  42.3 us
    all_to_all x1, blocking collectives, along(): lax.all_to_all(messages, ALL, 0, 0, axis_index_groups=lines(first), tiled...  20 us
    all_to_all x1, blocking collectives, shards(): got = lax.all_to_all(sliced, 'sp_1', 0, 0, tiled=True)  16.7 us
    ppermute x6, starting transfers between devices, shifted(): return lax.ppermute(own, 'tp_0', [(i, (i + d) % n) for i in range(n)])  16.5 us
    ppermute x5, starting transfers between devices, swapped(): return lax.ppermute(v, 'tp_1', [(0, 1), (1, 0)])  13.9 us
    all_to_all x1, blocking collectives, shards(): mine = lax.all_to_all(hidden, TP, 0, 0, tiled=True)  11 us
    all_to_all x1, waiting for transfers between devices, shards(): got = lax.all_to_all(row_end, 'sp_0', 0, 0, tiled=True)  7.73 us
    all_to_all x1, starting transfers between devices, along(): lax.all_to_all(messages, ALL, 0, 0, axis_index_groups=lines(first), tiled...  6.82 us
  transfers between devices with their start and end apart: 13, of which 8 were waited for; matrix products, arithmetic and copies ran while one was open for 1% of the time, Pallas kernels for 5%

commit v1 on v0

--- a/solution.py
+++ b/solution.py
@@ -140,8 +140,8 @@
 
 def project_kernel(place, rates, *refs):
     xs = refs[:8]
-    w_ref, cos_ref, sin_ref, q_hbm, k_hbm, v_hbm, p_hbm, o_hbm, s_out = refs[8:17]
-    x_buf, q_out, k_out, v_out, p_out, sems = refs[17:]
+    w_ref, cos_ref, sin_ref, q_hbm, k_hbm, v_hbm, p_hbm, o_hbm, s_hbm = refs[8:17]
+    x_buf, q_out, k_out, v_out, p_out, s_out, sems = refs[17:]
     core = place[1]
 
     cut = 3 * HEAD_DIM
@@ -222,6 +222,8 @@
     leaving.append(pltpu.make_async_copy(p_out, p_hbm, sems.at[3]))
     leaving[-1].start()
     write_message(s_out, state, jnp.exp(jnp.full((8, HEAD_DIM), -float(BLOCK), jnp.float32) * total))
+    leaving.append(pltpu.make_async_copy(s_out, s_hbm, sems.at[4]))
+    leaving[-1].start()
     for copy in leaving:
         copy.wait()
 
@@ -237,16 +239,17 @@
             rows,
             pltpu.HBM((8, HEAD_DIM, HEAD_DIM), jnp.bfloat16),
             pltpu.HBM((8, 8, 32, HEAD_DIM), jnp.bfloat16),
-            jax.ShapeDtypeStruct(MESSAGES, jnp.bfloat16),
+            pltpu.HBM(MESSAGES, jnp.bfloat16),
         ),
         in_specs=[SMEM, SMEM] + [ANY] * 8 + [VMEM] * 3,
-        out_specs=(HBM,) * 5 + (VMEM,),
+        out_specs=(HBM,) * 6,
         scratch_shapes=[
             pltpu.VMEM((span, 2048), jnp.bfloat16),
             pltpu.VMEM((span, HEAD_DIM), jnp.bfloat16),
             pltpu.VMEM((span, HEAD_DIM), jnp.bfloat16),
             pltpu.VMEM((span, HEAD_DIM), jnp.bfloat16),
             pltpu.VMEM((8, HEAD_DIM, HEAD_DIM), jnp.bfloat16),
+            pltpu.VMEM(MESSAGES, jnp.bfloat16),
             pltpu.SemaphoreType.DMA((10,)),
         ],
         compiler_params=pltpu.CompilerParams(vmem_limit_bytes=24 << 20),
@@ -257,6 +260,7 @@
 
 
 def local_kernel(rates, q_hbm, k_hbm, v_hbm, p_hbm, l_hbm, q_ref, k_ref, v_ref, p_ref, l_out, sems):
+    leaving = []
     pairs = ((q_hbm, q_ref), (k_hbm, k_ref), (v_hbm, v_ref), (p_hbm, p_ref))
     copies = [pltpu.make_async_copy(a, b, sems.at[j]) for j, (a, b) in enumerate(pairs)]
     for copy in copies:
@@ -279,16 +283,17 @@
         if b > 0:
             cross = jnp.dot(q, p_ref[b], preferred_element_type=jnp.float32)
             out = out + cross * jnp.exp(-(row + 1.0) * rate)
-        l_out[rows, :] = out
-    leaving = pltpu.make_async_copy(l_out, l_hbm, sems.at[4])
-    leaving.start()
-    leaving.wait()
+        l_out[rows, :] = out.astype(jnp.bfloat16)
+        leaving.append(pltpu.make_async_copy(l_out.at[rows], l_hbm.at[rows], sems.at[4 + b]))
+        leaving[-1].start()
+    for copy in leaving:
+        copy.wait()
 
 
 def local_part(rates, q, k, v, before):
     return pl.pallas_call(
         local_kernel,
-        out_shape=pltpu.HBM(q.shape, jnp.float32),
+        out_shape=pltpu.HBM(q.shape, jnp.bfloat16),
         in_specs=[SMEM] + [ANY] * 4,
         out_specs=HBM,
         scratch_shapes=[
@@ -296,8 +301,8 @@
             pltpu.VMEM(q.shape, jnp.bfloat16),
             pltpu.VMEM(q.shape, jnp.bfloat16),
             pltpu.VMEM(before.shape, jnp.bfloat16),
-            pltpu.VMEM(q.shape, jnp.float32),
-            pltpu.SemaphoreType.DMA((5,)),
+            pltpu.VMEM(q.shape, jnp.bfloat16),
+            pltpu.SemaphoreType.DMA((12,)),
         ],
         compiler_params=pltpu.CompilerParams(vmem_limit_bytes=4 << 20),
         cost_estimate=pl.CostEstimate(
@@ -347,7 +352,7 @@
         rate = rates[b, 0]
         rows = pl.ds(b * BLOCK, BLOCK)
         carried = jnp.dot(q_ref[rows, :], state, preferred_element_type=jnp.float32)
-        mixed = l_ref[rows, :] + carried * jnp.exp(-(row + 1.0) * rate - BLOCK * before)
+        mixed = l_ref[rows, :].astype(jnp.float32) + carried * jnp.exp(-(row + 1.0) * rate - BLOCK * before)
         norm = lax.rsqrt(jnp.mean(mixed * mixed, axis=-1, keepdims=True) + EPS)
         out_ref[b] = (mixed * norm * gain).astype(jnp.bfloat16)
         before = before + rate
@@ -361,7 +366,7 @@
         out_specs=VMEM,
         scratch_shapes=[
             pltpu.VMEM((8 * BLOCK, HEAD_DIM), jnp.bfloat16),
-            pltpu.VMEM((8 * BLOCK, HEAD_DIM), jnp.float32),
+            pltpu.VMEM((8 * BLOCK, HEAD_DIM), jnp.bfloat16),
             pltpu.VMEM((HEAD_DIM, HEAD_DIM), jnp.float32),
             pltpu.SemaphoreType.DMA((3,)),
         ],
@@ -372,28 +377,41 @@
     )(*args)
 
 
-def out_kernel(place, h_ref, same_ref, other_hbm, out_ref, other_buf, sems):
+def head_product(h_ref, w, place, j, own):
+    here = lax.rem(place[0] - j + 4, 4)
+    core = place[1] if own else 1 - place[1]
+    return lax.dot_general(
+        h_ref[here * 2 + core], w, (((1,), (1,)), ((), ())), preferred_element_type=jnp.float32
+    )
+
+
+def own_kernel(place, h_ref, same_ref, out_ref):
+    out_ref[...] = sum(head_product(h_ref, same_ref[j], place, j, True) for j in range(4))
+
+
+def out_kernel(place, h_ref, partial_ref, other_hbm, out_ref, other_buf, sems):
     copies = []
     for j in range(4):
         copies.append(pltpu.make_async_copy(other_hbm.at[j], other_buf.at[j], sems.at[j]))
         copies[-1].start()
-    total = None
-    for j in range(8):
-        here = lax.rem(place[0] - j % 4 + 4, 4)
-        core = place[1] if j < 4 else 1 - place[1]
-        if j >= 4:
-            copies[j - 4].wait()
-        part = lax.dot_general(
-            h_ref[here * 2 + core],
-            same_ref[j] if j < 4 else other_buf[j - 4],
-            (((1,), (1,)), ((), ())),
-            preferred_element_type=jnp.float32,
-        )
-        total = part if total is None else total + part
+    total = partial_ref[...]
+    for j in range(4):
+        copies[j].wait()
+        total = total + head_product(h_ref, other_buf[j], place, j, False)
     out_ref[...] = total.astype(jnp.bfloat16)
 
 
 def out_part(place, hidden, same, other):
+    partial = pl.pallas_call(
+        own_kernel,
+        out_shape=jax.ShapeDtypeStruct((BLOCK, 2048), jnp.float32),
+        in_specs=[SMEM, VMEM, VMEM],
+        out_specs=VMEM,
+        compiler_params=pltpu.CompilerParams(vmem_limit_bytes=8 << 20),
+        cost_estimate=pl.CostEstimate(
+            flops=270000000, bytes_accessed=3 << 20, transcendentals=0
+        ),
+    )(place, hidden, same)
     return pl.pallas_call(
         out_kernel,
         out_shape=jax.ShapeDtypeStruct((BLOCK, 2048), jnp.bfloat16),
@@ -403,11 +421,11 @@
             pltpu.VMEM((4, 2048, HEAD_DIM), jnp.bfloat16),
             pltpu.SemaphoreType.DMA((4,)),
         ],
-        compiler_params=pltpu.CompilerParams(vmem_limit_bytes=24 << 20),
+        compiler_params=pltpu.CompilerParams(vmem_limit_bytes=16 << 20),
         cost_estimate=pl.CostEstimate(
-            flops=540000000, bytes_accessed=5 << 20, transcendentals=0
-        ),
-    )(place, hidden, same, other)
+            flops=270000000, bytes_accessed=4 << 20, transcendentals=0
+        ),
+    )(place, hidden, partial, other)
 
 
 def rotation_tables(first, rows):

time: 169 us -> 170 us (level)
    pallas_call x1 -> x2, Pallas kernels: 3.29 us -> 4.42 us  [the longest x1 3.18 us: local_part(): pl.pallas_call(local_kernel, out_shape=pltpu.HBM(q.shape, jnp.bfloat16),...]
  transfers between devices with their start and end apart: 13 -> 13, of which waited for: 8 -> 8; matrix products, arithmetic and copies ran while one was open for 1% -> 1% of each run, Pallas kernels for 5% -> 6%
where the time goes in v1:
time: 170 us
  waiting for transfers between devices  52.2 us (31%)
  blocking collectives  47.7 us (28%)
  starting transfers between devices  42.8 us (25%)
  Pallas kernels  21.1 us (12%)
  other arithmetic  3.08 us (2%)
  local copies, waits for them, and re-layouts  2.43 us (1%)
    ppermute x6, waiting for transfers between devices, shifted(): return lax.ppermute(own, 'tp_0', [(i, (i + d) % n) for i in range(n)])  42.3 us
    all_to_all x1, blocking collectives, along(): lax.all_to_all(messages, ALL, 0, 0, axis_index_groups=lines(first), tiled...  20 us
    all_to_all x1, blocking collectives, shards(): got = lax.all_to_all(sliced, 'sp_1', 0, 0, tiled=True)  16.7 us
    ppermute x6, starting transfers between devices, shifted(): return lax.ppermute(own, 'tp_0', [(i, (i + d) % n) for i in range(n)])  16.7 us
    ppermute x5, starting transfers between devices, swapped(): return lax.ppermute(v, 'tp_1', [(0, 1), (1, 0)])  13.9 us
    all_to_all x1, blocking collectives, shards(): mine = lax.all_to_all(hidden, TP, 0, 0, tiled=True)  11 us
    all_to_all x1, waiting for transfers between devices, shards(): got = lax.all_to_all(row_end, 'sp_0', 0, 0, tiled=True)  7.84 us
    all_to_all x1, starting transfers between devices, along(): lax.all_to_all(messages, ALL, 0, 0, axis_index_groups=lines(first), tiled...  6.82 us
  transfers between devices with their start and end apart: 13, of which 8 were waited for; matrix products, arithmetic and copies ran while one was open for 1% of the time, Pallas kernels for 6%

profile of v1, /device:TPU:1, one launch (start us, length us, event | category | flops | bytes accessed | tf_op | source)
XLA Modules:
  0.0 169.5 jit_solution(5105763929508946848)
XLA Ops:
  0.8 20.0 %all_to_all.25 = bf16[8,32,512]{2,1,0:T(8,128)(2,1)S(1)} all-to-all(bf16[8,32,512]{2,1,0:T(8,128)(2,1)S(1)} %broadcast_in_dim.22), channel_id=1, replica_groups={{0,8,16,24,32,40,48,56},{2,10,18,26,34,42,50,58},{4,12,20,28,36,44,52,6..., dimensions={0} | all-to-all | bytes 524288 | tf_op jit(solution)/shard_map/all_to_all | solution.py:40
  20.8 1.5 broadcast_in_dim.24
  22.3 6.8 %all-to-all-start.1 = ((bf16[8,256,512]{2,1,0:T(8,128)(2,1)}), bf16[8,256,512]{2,1,0:T(8,128)(2,1)S(1)}, u32[]{:S(2)}, u32[]{:S(2)}) async-start(bf16[8,256,512]{2,1,0:T(8,128)(2,1)} %broadcast_in_dim.24), calls=%async_computation.1 | async-start | bytes 4194304 | tf_op jit(solution)/shard_map/all_to_all | solution.py:40
  29.1 2.1 %shard_map.91.refs_0_ = bf16[128,2048]{1,0:T(8,128)(2,1)} custom-call(bf16[128,2048]{1,0:T(8,128)(2,1)} %x_hbm.1, f32[1,2048]{1,0:T(1,128)} %bitcast.19), custom_call_target="tpu_custom_call" | custom-call | flops 2000000 | bytes 1048576 | tf_op jit(solution)/shard_map/pallas_call | solution.py:100
  31.2 4.3 %collective-permute-start.3 = (bf16[128,2048]{1,0:T(8,128)(2,1)}, bf16[128,2048]{1,0:T(8,128)(2,1)}, u32[]{:S(2)}, u32[]{:S(2)}) collective-permute-start(bf16[128,2048]{1,0:T(8,128)(2,1)} %shard_map.91.refs_0_), channel_id=1, source_target_pairs={{0,1},{1,0},{2,3},{3,2},{4,5},{5,4},{6,7},{7,6},{8,9},{9,8},{10,11... | collective-permute-start | bytes 1572872 | tf_op jit(solution)/shard_map/ppermute | solution.py:49
  35.5 4.4 %collective-permute-start.2 = (bf16[128,2048]{1,0:T(8,128)(2,1)}, bf16[128,2048]{1,0:T(8,128)(2,1)}, u32[]{:S(2)}, u32[]{:S(2)}) collective-permute-start(bf16[128,2048]{1,0:T(8,128)(2,1)} %shard_map.91.refs_0_), channel_id=1, source_target_pairs={{0,6},{2,0},{4,2},{6,4},{1,7},{3,1},{5,3},{7,5},{8,14},{10,8},{12,... | collective-permute-start | bytes 1572872 | tf_op jit(solution)/shard_map/ppermute | solution.py:45
  39.9 2.4 %collective-permute-start.1 = (bf16[128,2048]{1,0:T(8,128)(2,1)}, bf16[128,2048]{1,0:T(8,128)(2,1)}, u32[]{:S(2)}, u32[]{:S(2)}) collective-permute-start(bf16[128,2048]{1,0:T(8,128)(2,1)} %shard_map.91.refs_0_), channel_id=1, source_target_pairs={{0,4},{2,6},{4,0},{6,2},{1,5},{3,7},{5,1},{7,3},{8,12},{10,14},{12... | collective-permute-start | bytes 1572872 | tf_op jit(solution)/shard_map/ppermute | solution.py:45
  42.3 2.5 %collective-permute-start = (bf16[128,2048]{1,0:T(8,128)(2,1)}, bf16[128,2048]{1,0:T(8,128)(2,1)}, u32[]{:S(2)}, u32[]{:S(2)}) collective-permute-start(bf16[128,2048]{1,0:T(8,128)(2,1)} %shard_map.91.refs_0_), channel_id=1, source_target_pairs={{0,2},{2,4},{4,6},{6,0},{1,3},{3,5},{5,7},{7,1},{8,10},{10,12},{12... | collective-permute-start | bytes 1572872 | tf_op jit(solution)/shard_map/ppermute | solution.py:45
  44.9 1.9 %fusion = (f32[1024,64]{1,0:T(8,128)S(1)}, f32[1024,64]{1,0:T(8,128)S(1)}, f32[1024,64]{1,0:T(8,128)S(1)}) fusion(f32[64]{0:T(128)S(1)} %multiply_power_fusion, f32[1024]{0:T(1024)S(1)} %add_convert_fusion), kind=kLoop, calls=%fused_computation.4 | loop fusion | flops 131072 | bytes 790784 | tf_op jit(solution)/shard_map/neg | solution.py:439
  47.1 9.7 %collective-permute-done.1.refs_2_ = bf16[128,2048]{1,0:T(8,128)(2,1)} collective-permute-done((bf16[128,2048]{1,0:T(8,128)(2,1)}, bf16[128,2048]{1,0:T(8,128)(2,1)}, u32[]{:S(2)}, u32[]{:S(2)}) %collective-permute-start.1) | collective-permute-done | bytes 524320 | tf_op jit(solution)/shard_map/ppermute | solution.py:45
  56.8 5.7 %collective-permute-done.2.refs_3_ = bf16[128,2048]{1,0:T(8,128)(2,1)} collective-permute-done((bf16[128,2048]{1,0:T(8,128)(2,1)}, bf16[128,2048]{1,0:T(8,128)(2,1)}, u32[]{:S(2)}, u32[]{:S(2)}) %collective-permute-start.2) | collective-permute-done | bytes 524320 | tf_op jit(solution)/shard_map/ppermute | solution.py:45
  62.5 2.9 %collective-permute-start.6 = (bf16[128,2048]{1,0:T(8,128)(2,1)}, bf16[128,2048]{1,0:T(8,128)(2,1)}, u32[]{:S(2)}, u32[]{:S(2)}) collective-permute-start(bf16[128,2048]{1,0:T(8,128)(2,1)} %collective-permute-done.2.refs_3_), channel_id=1, source_target_pairs={{0,1},{1,0},{2,3},{3,2},{4,5},{5,4},{6,7},{7,6},{8,9},{9,8},{10,11... | collective-permute-start | bytes 1572872 | tf_op jit(solution)/shard_map/ppermute | solution.py:49
  65.5 3.2 %collective-permute-done.refs_1_ = bf16[128,2048]{1,0:T(8,128)(2,1)} collective-permute-done((bf16[128,2048]{1,0:T(8,128)(2,1)}, bf16[128,2048]{1,0:T(8,128)(2,1)}, u32[]{:S(2)}, u32[]{:S(2)}) %collective-permute-start) | collective-permute-done | bytes 524320 | tf_op jit(solution)/shard_map/ppermute | solution.py:45
  68.7 2.4 %collective-permute-start.4 = (bf16[128,2048]{1,0:T(8,128)(2,1)}, bf16[128,2048]{1,0:T(8,128)(2,1)}, u32[]{:S(2)}, u32[]{:S(2)}) collective-permute-start(bf16[128,2048]{1,0:T(8,128)(2,1)} %collective-permute-done.refs_1_), channel_id=1, source_target_pairs={{0,1},{1,0},{2,3},{3,2},{4,5},{5,4},{6,7},{7,6},{8,9},{9,8},{10,11... | collective-permute-start | bytes 1572872 | tf_op jit(solution)/shard_map/ppermute | solution.py:49
  71.1 1.9 %collective-permute-start.5 = (bf16[128,2048]{1,0:T(8,128)(2,1)}, bf16[128,2048]{1,0:T(8,128)(2,1)}, u32[]{:S(2)}, u32[]{:S(2)}) collective-permute-start(bf16[128,2048]{1,0:T(8,128)(2,1)} %collective-permute-done.1.refs_2_), channel_id=1, source_target_pairs={{0,1},{1,0},{2,3},{3,2},{4,5},{5,4},{6,7},{7,6},{8,9},{9,8},{10,11... | collective-permute-start | bytes 1572872 | tf_op jit(solution)/shard_map/ppermute | solution.py:49
  73.2 2.0 %collective-permute-done.5.refs_6_ = bf16[128,2048]{1,0:T(8,128)(2,1)} collective-permute-done((bf16[128,2048]{1,0:T(8,128)(2,1)}, bf16[128,2048]{1,0:T(8,128)(2,1)}, u32[]{:S(2)}, u32[]{:S(2)}) %collective-permute-start.5) | collective-permute-done | bytes 524320 | tf_op jit(solution)/shard_map/ppermute | solution.py:49
  75.2 6.3 %shard_map.92 = (bf16[1024,128]{1,0:T(8,128)(2,1)}, bf16[1024,128]{1,0:T(8,128)(2,1)}, bf16[1024,128]{1,0:T(8,128)(2,1)}, bf16[8,128,128]{2,1,0:T(8,128)(2,1)}, ...) custom-call(s32[4]{0:T(128)S(1)} %pad_add_fusion.place, f32[8,1]{1,0:T(8,128)S(1)} %copy.12.rates, ...), custom_call_target="tpu_custom_call" | custom-call | flops 1700000000 | bytes 7340032 | tf_op jit(solution)/shard_map/pallas_call | solution.py:234
  81.6 2.4 %collective-permute-start.9 = (bf16[2048,128]{1,0:T(8,128)(2,1)}, bf16[2048,128]{1,0:T(8,128)(2,1)S(1)}, u32[]{:S(2)}, u32[]{:S(2)}) collective-permute-start(bf16[2048,128]{1,0:T(8,128)(2,1)} %bitcast.14), channel_id=1, source_target_pairs={{0,6},{2,0},{4,2},{6,4},{1,7},{3,1},{5,3},{7,5},{8,14},{10,8},{12,... | collective-permute-start | bytes 1572872 | tf_op jit(solution)/shard_map/ppermute | solution.py:45
  84.0 2.4 %collective-permute-start.8 = (bf16[2048,128]{1,0:T(8,128)(2,1)}, bf16[2048,128]{1,0:T(8,128)(2,1)S(1)}, u32[]{:S(2)}, u32[]{:S(2)}) collective-permute-start(bf16[2048,128]{1,0:T(8,128)(2,1)} %bitcast.15), channel_id=1, source_target_pairs={{0,4},{2,6},{4,0},{6,2},{1,5},{3,7},{5,1},{7,3},{8,12},{10,14},{12... | collective-permute-start | bytes 1572872 | tf_op jit(solution)/shard_map/ppermute | solution.py:45
  86.4 2.5 %collective-permute-start.7 = (bf16[2048,128]{1,0:T(8,128)(2,1)}, bf16[2048,128]{1,0:T(8,128)(2,1)S(1)}, u32[]{:S(2)}, u32[]{:S(2)}) collective-permute-start(bf16[2048,128]{1,0:T(8,128)(2,1)} %bitcast.16), channel_id=1, source_target_pairs={{0,2},{2,4},{4,6},{6,0},{1,3},{3,5},{5,7},{7,1},{8,10},{10,12},{12... | collective-permute-start | bytes 1572872 | tf_op jit(solution)/shard_map/ppermute | solution.py:45
  88.9 8.2 %collective-permute-done.9.refs_3_ = bf16[2048,128]{1,0:T(8,128)(2,1)S(1)} collective-permute-done((bf16[2048,128]{1,0:T(8,128)(2,1)}, bf16[2048,128]{1,0:T(8,128)(2,1)S(1)}, u32[]{:S(2)}, u32[]{:S(2)}) %collective-permute-start.9) | collective-permute-done | bytes 524320 | tf_op jit(solution)/shard_map/ppermute | solution.py:45
  97.2 3.5 %collective-permute-done.8.refs_2_ = bf16[2048,128]{1,0:T(8,128)(2,1)S(1)} collective-permute-done((bf16[2048,128]{1,0:T(8,128)(2,1)}, bf16[2048,128]{1,0:T(8,128)(2,1)S(1)}, u32[]{:S(2)}, u32[]{:S(2)}) %collective-permute-start.8) | collective-permute-done | bytes 524320 | tf_op jit(solution)/shard_map/ppermute | solution.py:45
  100.7 12.0 %collective-permute-done.7.refs_1_ = bf16[2048,128]{1,0:T(8,128)(2,1)S(1)} collective-permute-done((bf16[2048,128]{1,0:T(8,128)(2,1)}, bf16[2048,128]{1,0:T(8,128)(2,1)S(1)}, u32[]{:S(2)}, u32[]{:S(2)}) %collective-permute-start.7) | collective-permute-done | bytes 524320 | tf_op jit(solution)/shard_map/ppermute | solution.py:45
  113.5 1.5 shard_map.96.same_ref
  115.0 2.4 %collective-permute-start.10 = (bf16[4,2048,128]{2,1,0:T(8,128)(2,1)S(1)}, bf16[4,2048,128]{2,1,0:T(8,128)(2,1)}, u32[]{:S(2)}, u32[]{:S(2)}) collective-permute-start(bf16[4,2048,128]{2,1,0:T(8,128)(2,1)S(1)} %shard_map.96.same_ref), channel_id=1, source_target_pairs={{0,1},{1,0},{2,3},{3,2},{4,5},{5,4},{6,7},{7,6},{8,9},{9,8},{10,11... | collective-permute-start | bytes 6291464 | tf_op jit(solution)/shard_map/ppermute | solution.py:49
  117.4 16.7 %all_to_all.26.got = bf16[8,136,128]{2,1,0:T(8,128)(2,1)S(1)} all-to-all(bf16[8,136,128]{2,1,0:T(8,128)(2,1)S(1)} %copy-done.4), channel_id=1, replica_groups=mesh['sp_0'=8,'sp_1'=8,'tp_0'=4,'tp_1'=2] {'sp_1'}, dimensions={0} | all-to-all | bytes 557056 | tf_op jit(solution)/shard_map/all_to_all | solution.py:457
  135.5 5.4 %all-to-all-start.3 = ((bf16[8,136,128]{2,1,0:T(8,128)(2,1)}), bf16[8,136,128]{2,1,0:T(8,128)(2,1)S(1)}, u32[]{:S(2)}, u32[]{:S(2)}) async-start(bf16[8,136,128]{2,1,0:T(8,128)(2,1)} %get-tuple-element.21), calls=%async_computation.3 | async-start | bytes 557056 | tf_op jit(solution)/shard_map/all_to_all | solution.py:459
  140.8 3.2 %shard_map.94.l_hbm = bf16[1024,128]{1,0:T(8,128)(2,1)} custom-call(f32[8,1]{1,0:T(8,128)S(1)} %copy.12.rates, bf16[1024,128]{1,0:T(8,128)(2,1)} %get-tuple-element.24.q_hbm, bf16[1024,128]{1,0:T(8,128)(2,1)} %get-tuple-element.25.k_hbm, bf16[1024,128]{1,0:T(8,128)(2,1)} %get-tuple-element.26.v_hbm, bf16[8,128,128]{2,1,0:T(8,128)(2,1)} %get-tuple-element.27.p_hbm), custom_call_target="tpu_custom_call" | custom-call | flops 1000000000 | bytes 2097152 | tf_op jit(solution)/shard_map/pallas_call | solution.py:294
  144.0 7.8 %all-to-all-done.3.got = bf16[8,136,128]{2,1,0:T(8,128)(2,1)S(1)} async-done(((bf16[8,136,128]{2,1,0:T(8,128)(2,1)}), bf16[8,136,128]{2,1,0:T(8,128)(2,1)S(1)}, u32[]{:S(2)}, u32[]{:S(2)}) %all-to-all-start.3) | async-done | bytes 278560 | tf_op jit(solution)/shard_map/all_to_all | solution.py:459
  151.9 2.1 %shard_map.95 = bf16[8,128,128]{2,1,0:T(8,128)(2,1)S(1)} custom-call(s32[4]{0:T(128)S(1)} %pad_add_fusion.place, f32[8,1]{1,0:T(8,128)S(1)} %copy.12.rates, bf16[8,136,128]{2,1,0:T(8,128)(2,1)S(1)} %all-to-all-done.3.got, f32[128,128]{1,0:T(8,128)S(1)} %get-tuple-element.22.before_ref, f32[8,128]{1,0:T(8,128)S(1)} %get-tuple-element.23.shrunk_ref, ...), custom_call_target="tpu_custom_call" | custom-call | flops 40000000 | bytes 1048576 | tf_op jit(solution)/shard_map/pallas_call | solution.py:362
  153.9 11.0 %all_to_all.27.h_ref = bf16[8,128,128]{2,1,0:T(8,128)(2,1)S(1)} all-to-all(bf16[8,128,128]{2,1,0:T(8,128)(2,1)S(1)} %shard_map.95), channel_id=1, replica_groups=mesh['sp_0'=8,'sp_1'=8,'tp_0'=4,'tp_1'=2] {'tp_0','tp_1'}, dimensions={0} | all-to-all | bytes 524288 | tf_op jit(solution)/shard_map/all_to_all | solution.py:471
  166.2 3.3 %shard_map.98 = bf16[128,2048]{1,0:T(8,128)(2,1)} custom-call(s32[4]{0:T(128)S(1)} %pad_add_fusion.place, bf16[8,128,128]{2,1,0:T(8,128)(2,1)S(1)} %all_to_all.27.h_ref, f32[128,2048]{1,0:T(8,128)S(1)} %shard_map.97.partial_ref, bf16[4,2048,128]{2,1,0:T(8,128)(2,1)} %collective-permute-done.10.other_hbm), custom_call_target="tpu_custom_call" | custom-call | flops 270000000 | bytes 4194304 | tf_op jit(solution)/shard_map/pallas_call | solution.py:415
  (26 shorter events, 4.7 us)
Async XLA Ops:
  22.3 52.9 %all-to-all-start.1 = ((bf16[8,256,512]{2,1,0:T(8,128)(2,1)}), bf16[8,256,512]{2,1,0:T(8,128)(2,1)S(1)}, u32[]{:S(2)}, u32[]{:S(2)}) async-start(bf16[8,256,512]{2,1,0:T(8,128)(2,1)} %broadcast_in_dim.24), calls=%async_computation.1 | async-start | bytes 4194304 | tf_op jit(solution)/shard_map/all_to_all | solution.py:40
  31.2 42.0 %collective-permute-start.3 = (bf16[128,2048]{1,0:T(8,128)(2,1)}, bf16[128,2048]{1,0:T(8,128)(2,1)}, u32[]{:S(2)}, u32[]{:S(2)}) collective-permute-start(bf16[128,2048]{1,0:T(8,128)(2,1)} %shard_map.91.refs_0_), channel_id=1, source_target_pairs={{0,1},{1,0},{2,3},{3,2},{4,5},{5,4},{6,7},{7,6},{8,9},{9,8},{10,11... | collective-permute-start | bytes 1572872 | tf_op jit(solution)/shard_map/ppermute | solution.py:49
  35.5 27.0 %collective-permute-start.2 = (bf16[128,2048]{1,0:T(8,128)(2,1)}, bf16[128,2048]{1,0:T(8,128)(2,1)}, u32[]{:S(2)}, u32[]{:S(2)}) collective-permute-start(bf16[128,2048]{1,0:T(8,128)(2,1)} %shard_map.91.refs_0_), channel_id=1, source_target_pairs={{0,6},{2,0},{4,2},{6,4},{1,7},{3,1},{5,3},{7,5},{8,14},{10,8},{12,... | collective-permute-start | bytes 1572872 | tf_op jit(solution)/shard_map/ppermute | solution.py:45
  39.9 16.9 %collective-permute-start.1 = (bf16[128,2048]{1,0:T(8,128)(2,1)}, bf16[128,2048]{1,0:T(8,128)(2,1)}, u32[]{:S(2)}, u32[]{:S(2)}) collective-permute-start(bf16[128,2048]{1,0:T(8,128)(2,1)} %shard_map.91.refs_0_), channel_id=1, source_target_pairs={{0,4},{2,6},{4,0},{6,2},{1,5},{3,7},{5,1},{7,3},{8,12},{10,14},{12... | collective-permute-start | bytes 1572872 | tf_op jit(solution)/shard_map/ppermute | solution.py:45
  42.3 26.4 %collective-permute-start = (bf16[128,2048]{1,0:T(8,128)(2,1)}, bf16[128,2048]{1,0:T(8,128)(2,1)}, u32[]{:S(2)}, u32[]{:S(2)}) collective-permute-start(bf16[128,2048]{1,0:T(8,128)(2,1)} %shard_map.91.refs_0_), channel_id=1, source_target_pairs={{0,2},{2,4},{4,6},{6,0},{1,3},{3,5},{5,7},{7,1},{8,10},{10,12},{12... | collective-permute-start | bytes 1572872 | tf_op jit(solution)/shard_map/ppermute | solution.py:45
  44.9 28.1 %copy-start.5 = (f32[8,1]{0,1:T(1,128)S(1)}, f32[8,1]{0,1:T(1,128)}, u32[]{:S(2)}) copy-start(f32[8,1]{0,1:T(1,128)} %param.14) | copy-start | bytes 100
  62.5 10.7 %collective-permute-start.6 = (bf16[128,2048]{1,0:T(8,128)(2,1)}, bf16[128,2048]{1,0:T(8,128)(2,1)}, u32[]{:S(2)}, u32[]{:S(2)}) collective-permute-start(bf16[128,2048]{1,0:T(8,128)(2,1)} %collective-permute-done.2.refs_3_), channel_id=1, source_target_pairs={{0,1},{1,0},{2,3},{3,2},{4,5},{5,4},{6,7},{7,6},{8,9},{9,8},{10,11... | collective-permute-start | bytes 1572872 | tf_op jit(solution)/shard_map/ppermute | solution.py:49
  68.7 4.5 %collective-permute-start.4 = (bf16[128,2048]{1,0:T(8,128)(2,1)}, bf16[128,2048]{1,0:T(8,128)(2,1)}, u32[]{:S(2)}, u32[]{:S(2)}) collective-permute-start(bf16[128,2048]{1,0:T(8,128)(2,1)} %collective-permute-done.refs_1_), channel_id=1, source_target_pairs={{0,1},{1,0},{2,3},{3,2},{4,5},{5,4},{6,7},{7,6},{8,9},{9,8},{10,11... | collective-permute-start | bytes 1572872 | tf_op jit(solution)/shard_map/ppermute | solution.py:49
  71.1 4.1 %collective-permute-start.5 = (bf16[128,2048]{1,0:T(8,128)(2,1)}, bf16[128,2048]{1,0:T(8,128)(2,1)}, u32[]{:S(2)}, u32[]{:S(2)}) collective-permute-start(bf16[128,2048]{1,0:T(8,128)(2,1)} %collective-permute-done.1.refs_2_), channel_id=1, source_target_pairs={{0,1},{1,0},{2,3},{3,2},{4,5},{5,4},{6,7},{7,6},{8,9},{9,8},{10,11... | collective-permute-start | bytes 1572872 | tf_op jit(solution)/shard_map/ppermute | solution.py:49
  81.6 35.8 %copy-start.4 = (bf16[8,136,128]{2,1,0:T(8,128)(2,1)S(1)}, bf16[8,136,128]{2,1,0:T(8,128)(2,1)}, u32[]{:S(2)}) copy-start(bf16[8,136,128]{2,1,0:T(8,128)(2,1)} %get-tuple-element.20) | copy-start | bytes 835588
  81.6 15.6 %collective-permute-start.9 = (bf16[2048,128]{1,0:T(8,128)(2,1)}, bf16[2048,128]{1,0:T(8,128)(2,1)S(1)}, u32[]{:S(2)}, u32[]{:S(2)}) collective-permute-start(bf16[2048,128]{1,0:T(8,128)(2,1)} %bitcast.14), channel_id=1, source_target_pairs={{0,6},{2,0},{4,2},{6,4},{1,7},{3,1},{5,3},{7,5},{8,14},{10,8},{12,... | collective-permute-start | bytes 1572872 | tf_op jit(solution)/shard_map/ppermute | solution.py:45
  84.0 16.7 %collective-permute-start.8 = (bf16[2048,128]{1,0:T(8,128)(2,1)}, bf16[2048,128]{1,0:T(8,128)(2,1)S(1)}, u32[]{:S(2)}, u32[]{:S(2)}) collective-permute-start(bf16[2048,128]{1,0:T(8,128)(2,1)} %bitcast.15), channel_id=1, source_target_pairs={{0,4},{2,6},{4,0},{6,2},{1,5},{3,7},{5,1},{7,3},{8,12},{10,14},{12... | collective-permute-start | bytes 1572872 | tf_op jit(solution)/shard_map/ppermute | solution.py:45
  86.4 26.3 %collective-permute-start.7 = (bf16[2048,128]{1,0:T(8,128)(2,1)}, bf16[2048,128]{1,0:T(8,128)(2,1)S(1)}, u32[]{:S(2)}, u32[]{:S(2)}) collective-permute-start(bf16[2048,128]{1,0:T(8,128)(2,1)} %bitcast.16), channel_id=1, source_target_pairs={{0,2},{2,4},{4,6},{6,0},{1,3},{3,5},{5,7},{7,1},{8,10},{10,12},{12... | collective-permute-start | bytes 1572872 | tf_op jit(solution)/shard_map/ppermute | solution.py:45
  97.2 15.5 %copy-start.1 = (bf16[2048,128]{1,0:T(8,128)(2,1)}, bf16[2048,128]{1,0:T(8,128)(2,1)S(1)}, u32[]{:S(2)}) copy-start(bf16[2048,128]{1,0:T(8,128)(2,1)S(1)} %collective-permute-done.9.refs_3_) | copy-start | bytes 1572868
  100.7 12.0 %copy-start.2 = (bf16[2048,128]{1,0:T(8,128)(2,1)}, bf16[2048,128]{1,0:T(8,128)(2,1)S(1)}, u32[]{:S(2)}) copy-start(bf16[2048,128]{1,0:T(8,128)(2,1)S(1)} %collective-permute-done.8.refs_2_) | copy-start | bytes 1572868
  112.7 0.8 copy-start.3
  115.0 51.2 %collective-permute-start.10 = (bf16[4,2048,128]{2,1,0:T(8,128)(2,1)S(1)}, bf16[4,2048,128]{2,1,0:T(8,128)(2,1)}, u32[]{:S(2)}, u32[]{:S(2)}) collective-permute-start(bf16[4,2048,128]{2,1,0:T(8,128)(2,1)S(1)} %shard_map.96.same_ref), channel_id=1, source_target_pairs={{0,1},{1,0},{2,3},{3,2},{4,5},{5,4},{6,7},{7,6},{8,9},{9,8},{10,11... | collective-permute-start | bytes 6291464 | tf_op jit(solution)/shard_map/ppermute | solution.py:49
  135.5 16.4 %copy-start = (f32[128]{0:T(128)S(1)}, f32[128]{0:T(128)}, u32[]{:S(2)}) copy-start(f32[128]{0:T(128)} %param.16) | copy-start | bytes 1540
  135.5 16.4 %all-to-all-start.3 = ((bf16[8,136,128]{2,1,0:T(8,128)(2,1)}), bf16[8,136,128]{2,1,0:T(8,128)(2,1)S(1)}, u32[]{:S(2)}, u32[]{:S(2)}) async-start(bf16[8,136,128]{2,1,0:T(8,128)(2,1)} %get-tuple-element.21), calls=%async_computation.3 | async-start | bytes 557056 | tf_op jit(solution)/shard_map/all_to_all | solution.py:459

commit v2 on v1

--- a/solution.py
+++ b/solution.py
@@ -82,47 +82,59 @@
     return same, swapped(same)
 
 
-def norm_kernel(x_hbm, gain_hbm, out_ref, x_ref, gain_ref, sems):
-    copies = [
-        pltpu.make_async_copy(x_hbm, x_ref, sems.at[0]),
-        pltpu.make_async_copy(gain_hbm, gain_ref, sems.at[1]),
+def norm_kernel(x_hbm, gain_hbm, out_hbm, x_ref, gain_ref, out_ref, in_sems, out_sems, gain_sem):
+    pieces = [pl.ds(j * 32, 32) for j in range(4)]
+    arriving = [
+        pltpu.make_async_copy(x_hbm.at[p], x_ref.at[p], in_sems.at[j]) for j, p in enumerate(pieces)
     ]
-    for copy in copies:
+    gain_copy = pltpu.make_async_copy(gain_hbm, gain_ref, gain_sem)
+    gain_copy.start()
+    for copy in arriving:
         copy.start()
-    for copy in copies:
+    gain_copy.wait()
+    leaving = []
+    for j, p in enumerate(pieces):
+        arriving[j].wait()
+        x = x_ref[p, :].astype(jnp.float32)
+        scale = lax.rsqrt(jnp.mean(x * x, axis=-1, keepdims=True) + EPS)
+        out_ref[p, :] = (x * scale * gain_ref[...]).astype(jnp.bfloat16)
+        leaving.append(pltpu.make_async_copy(out_ref.at[p], out_hbm.at[p], out_sems.at[j]))
+        leaving[-1].start()
+    for copy in leaving:
         copy.wait()
-    x = x_ref[...].astype(jnp.float32)
-    scale = lax.rsqrt(jnp.mean(x * x, axis=-1, keepdims=True) + EPS)
-    out_ref[...] = (x * scale * gain_ref[...]).astype(jnp.bfloat16)
 
 
 def normalized(tokens, gain):
     return pl.pallas_call(
         norm_kernel,
-        out_shape=jax.ShapeDtypeStruct(tokens.shape, jnp.bfloat16),
+        out_shape=pltpu.HBM(tokens.shape, jnp.bfloat16),
         in_specs=[ANY, ANY],
-        out_specs=VMEM,
+        out_specs=HBM,
         scratch_shapes=[
             pltpu.VMEM(tokens.shape, tokens.dtype),
             pltpu.VMEM((1, tokens.shape[1]), gain.dtype),
-            pltpu.SemaphoreType.DMA((2,)),
+            pltpu.VMEM(tokens.shape, jnp.bfloat16),
+            pltpu.SemaphoreType.DMA((4,)),
+            pltpu.SemaphoreType.DMA((4,)),
+            pltpu.SemaphoreType.DMA,
         ],
         compiler_params=pltpu.CompilerParams(vmem_limit_bytes=8 << 20),
         cost_estimate=pl.CostEstimate(flops=2000000, bytes_accessed=1 << 20, transcendentals=0),
     )(in_hbm(tokens), in_hbm(gain[None]))
 
 
-def write_message(out, state, decay):
+def write_message(message, out, sem, state, decay):
     row = lax.broadcasted_iota(jnp.int32, (8, HEAD_DIM), 0)
     high = decay.astype(jnp.bfloat16).astype(jnp.float32)
     rest = decay - high
     middle = rest.astype(jnp.bfloat16).astype(jnp.float32)
     addends = jnp.where(row == 0, high, jnp.where(row == 1, middle, rest - middle))
-    addends = jnp.where(row < 3, addends, 0.0).astype(jnp.bfloat16)
-    state = state.astype(jnp.bfloat16)
-    for i in range(8):
-        out[i, 0:HEAD_DIM, :] = state
-        out[i, HEAD_DIM : HEAD_DIM + 8, :] = addends
+    message[0:HEAD_DIM, :] = state.astype(jnp.bfloat16)
+    message[HEAD_DIM : HEAD_DIM + 8, :] = jnp.where(row < 3, addends, 0.0).astype(jnp.bfloat16)
+    copies = [pltpu.make_async_copy(message, out.at[i], sem.at[i]) for i in range(8)]
+    for copy in copies:
+        copy.start()
+    return copies
 
 
 def carried_on(got, here, state):
@@ -221,9 +233,8 @@
         state = jnp.exp(jnp.full((HEAD_DIM, HEAD_DIM), -float(BLOCK), jnp.float32) * rate) * state + kv
     leaving.append(pltpu.make_async_copy(p_out, p_hbm, sems.at[3]))
     leaving[-1].start()
-    write_message(s_out, state, jnp.exp(jnp.full((8, HEAD_DIM), -float(BLOCK), jnp.float32) * total))
-    leaving.append(pltpu.make_async_copy(s_out, s_hbm, sems.at[4]))
-    leaving[-1].start()
+    decay = jnp.exp(jnp.full((8, HEAD_DIM), -float(BLOCK), jnp.float32) * total)
+    leaving += write_message(s_out, s_hbm, sems.at[pl.ds(10, 8)], state, decay)
     for copy in leaving:
         copy.wait()
 
@@ -249,8 +260,8 @@
             pltpu.VMEM((span, HEAD_DIM), jnp.bfloat16),
             pltpu.VMEM((span, HEAD_DIM), jnp.bfloat16),
             pltpu.VMEM((8, HEAD_DIM, HEAD_DIM), jnp.bfloat16),
-            pltpu.VMEM(MESSAGES, jnp.bfloat16),
-            pltpu.SemaphoreType.DMA((10,)),
+            pltpu.VMEM(MESSAGES[1:], jnp.bfloat16),
+            pltpu.SemaphoreType.DMA((18,)),
         ],
         compiler_params=pltpu.CompilerParams(vmem_limit_bytes=24 << 20),
         cost_estimate=pl.CostEstimate(
@@ -311,24 +322,30 @@
     )(rates, q, k, v, before)
 
 
-def row_kernel(place, got, out, before_out, shrunk_out):
+def row_kernel(place, got, out, before_out, shrunk_out, message, sems):
     zero = jnp.zeros((HEAD_DIM, HEAD_DIM), jnp.float32)
     before, shrunk, end, passed = carried_on(got, place[3], zero)
-    write_message(out, end, jnp.broadcast_to(passed, (8, HEAD_DIM)))
+    copies = write_message(message, out, sems, end, jnp.broadcast_to(passed, (8, HEAD_DIM)))
     before_out[...] = before
     shrunk_out[...] = jnp.broadcast_to(shrunk, (8, HEAD_DIM))
+    for copy in copies:
+        copy.wait()
 
 
 def along_row(place, got):
     return pl.pallas_call(
         row_kernel,
         out_shape=(
-            jax.ShapeDtypeStruct(MESSAGES, jnp.bfloat16),
+            pltpu.HBM(MESSAGES, jnp.bfloat16),
             jax.ShapeDtypeStruct((HEAD_DIM, HEAD_DIM), jnp.float32),
             jax.ShapeDtypeStruct((8, HEAD_DIM), jnp.float32),
         ),
         in_specs=[SMEM, VMEM],
-        out_specs=(VMEM,) * 3,
+        out_specs=(HBM, VMEM, VMEM),
+        scratch_shapes=[
+            pltpu.VMEM(MESSAGES[1:], jnp.bfloat16),
+            pltpu.SemaphoreType.DMA((8,)),
+        ],
         compiler_params=pltpu.CompilerParams(vmem_limit_bytes=2 << 20),
         cost_estimate=pl.CostEstimate(flops=1000000, bytes_accessed=1 << 18, transcendentals=0),
     )(place, got)

time: 170 us -> 171 us (level)
  no operation moved by 1% of the time
where the time goes in v2:
time: 171 us
  waiting for transfers between devices  52.2 us (31%)
  blocking collectives  47.7 us (28%)
  starting transfers between devices  42.7 us (25%)
  Pallas kernels  21.1 us (12%)
  local copies, waits for them, and re-layouts  3.49 us (2%)
  other arithmetic  3.08 us (2%)
    ppermute x6, waiting for transfers between devices, shifted(): return lax.ppermute(own, 'tp_0', [(i, (i + d) % n) for i in range(n)])  42.3 us
    all_to_all x1, blocking collectives, along(): lax.all_to_all(messages, ALL, 0, 0, axis_index_groups=lines(first), tiled...  20 us
    all_to_all x1, blocking collectives, shards(): got = lax.all_to_all(sliced, 'sp_1', 0, 0, tiled=True)  16.7 us
    ppermute x6, starting transfers between devices, shifted(): return lax.ppermute(own, 'tp_0', [(i, (i + d) % n) for i in range(n)])  16.7 us
    ppermute x5, starting transfers between devices, swapped(): return lax.ppermute(v, 'tp_1', [(0, 1), (1, 0)])  13.9 us
    all_to_all x1, blocking collectives, shards(): mine = lax.all_to_all(hidden, TP, 0, 0, tiled=True)  11 us
    all_to_all x1, waiting for transfers between devices, shards(): got = lax.all_to_all(row_end, 'sp_0', 0, 0, tiled=True)  7.86 us
    all_to_all x1, starting transfers between devices, along(): lax.all_to_all(messages, ALL, 0, 0, axis_index_groups=lines(first), tiled...  6.82 us
  transfers between devices with their start and end apart: 13, of which 8 were waited for; matrix products, arithmetic and copies ran while one was open for 1% of the time, Pallas kernels for 6%

profile of v2, /device:TPU:1, one launch (start us, length us, event | category | flops | bytes accessed | tf_op | source)
XLA Modules:
  0.0 170.5 jit_solution(7799121180520439051)
XLA Ops:
  0.8 20.0 %all_to_all.25 = bf16[8,32,512]{2,1,0:T(8,128)(2,1)S(1)} all-to-all(bf16[8,32,512]{2,1,0:T(8,128)(2,1)S(1)} %broadcast_in_dim.22), channel_id=1, replica_groups={{0,8,16,24,32,40,48,56},{2,10,18,26,34,42,50,58},{4,12,20,28,36,44,52,6..., dimensions={0} | all-to-all | bytes 524288 | tf_op jit(solution)/shard_map/all_to_all | solution.py:40
  20.8 1.5 broadcast_in_dim.24
  22.3 6.8 %all-to-all-start.1 = ((bf16[8,256,512]{2,1,0:T(8,128)(2,1)}), bf16[8,256,512]{2,1,0:T(8,128)(2,1)S(1)}, u32[]{:S(2)}, u32[]{:S(2)}) async-start(bf16[8,256,512]{2,1,0:T(8,128)(2,1)} %broadcast_in_dim.24), calls=%async_computation.1 | async-start | bytes 4194304 | tf_op jit(solution)/shard_map/all_to_all | solution.py:40
  29.1 2.1 %shard_map.91.refs_0_ = bf16[128,2048]{1,0:T(8,128)(2,1)} custom-call(bf16[128,2048]{1,0:T(8,128)(2,1)} %x_hbm.1, f32[1,2048]{1,0:T(1,128)} %bitcast.19), custom_call_target="tpu_custom_call" | custom-call | flops 2000000 | bytes 1048576 | tf_op jit(solution)/shard_map/pallas_call | solution.py:108
  31.3 4.3 %collective-permute-start.3 = (bf16[128,2048]{1,0:T(8,128)(2,1)}, bf16[128,2048]{1,0:T(8,128)(2,1)}, u32[]{:S(2)}, u32[]{:S(2)}) collective-permute-start(bf16[128,2048]{1,0:T(8,128)(2,1)} %shard_map.91.refs_0_), channel_id=1, source_target_pairs={{0,1},{1,0},{2,3},{3,2},{4,5},{5,4},{6,7},{7,6},{8,9},{9,8},{10,11... | collective-permute-start | bytes 1572872 | tf_op jit(solution)/shard_map/ppermute | solution.py:49
  35.6 4.4 %collective-permute-start.2 = (bf16[128,2048]{1,0:T(8,128)(2,1)}, bf16[128,2048]{1,0:T(8,128)(2,1)}, u32[]{:S(2)}, u32[]{:S(2)}) collective-permute-start(bf16[128,2048]{1,0:T(8,128)(2,1)} %shard_map.91.refs_0_), channel_id=1, source_target_pairs={{0,6},{2,0},{4,2},{6,4},{1,7},{3,1},{5,3},{7,5},{8,14},{10,8},{12,... | collective-permute-start | bytes 1572872 | tf_op jit(solution)/shard_map/ppermute | solution.py:45
  40.0 2.4 %collective-permute-start.1 = (bf16[128,2048]{1,0:T(8,128)(2,1)}, bf16[128,2048]{1,0:T(8,128)(2,1)}, u32[]{:S(2)}, u32[]{:S(2)}) collective-permute-start(bf16[128,2048]{1,0:T(8,128)(2,1)} %shard_map.91.refs_0_), channel_id=1, source_target_pairs={{0,4},{2,6},{4,0},{6,2},{1,5},{3,7},{5,1},{7,3},{8,12},{10,14},{12... | collective-permute-start | bytes 1572872 | tf_op jit(solution)/shard_map/ppermute | solution.py:45
  42.4 2.5 %collective-permute-start = (bf16[128,2048]{1,0:T(8,128)(2,1)}, bf16[128,2048]{1,0:T(8,128)(2,1)}, u32[]{:S(2)}, u32[]{:S(2)}) collective-permute-start(bf16[128,2048]{1,0:T(8,128)(2,1)} %shard_map.91.refs_0_), channel_id=1, source_target_pairs={{0,2},{2,4},{4,6},{6,0},{1,3},{3,5},{5,7},{7,1},{8,10},{10,12},{12... | collective-permute-start | bytes 1572872 | tf_op jit(solution)/shard_map/ppermute | solution.py:45
  45.0 1.9 %fusion = (f32[1024,64]{1,0:T(8,128)S(1)}, f32[1024,64]{1,0:T(8,128)S(1)}, f32[1024,64]{1,0:T(8,128)S(1)}) fusion(f32[64]{0:T(128)S(1)} %multiply_power_fusion, f32[1024]{0:T(1024)S(1)} %add_convert_fusion), kind=kLoop, calls=%fused_computation.4 | loop fusion | flops 131072 | bytes 790784 | tf_op jit(solution)/shard_map/neg | solution.py:456
  47.2 9.7 %collective-permute-done.1.refs_2_ = bf16[128,2048]{1,0:T(8,128)(2,1)} collective-permute-done((bf16[128,2048]{1,0:T(8,128)(2,1)}, bf16[128,2048]{1,0:T(8,128)(2,1)}, u32[]{:S(2)}, u32[]{:S(2)}) %collective-permute-start.1) | collective-permute-done | bytes 524320 | tf_op jit(solution)/shard_map/ppermute | solution.py:45
  56.9 5.7 %collective-permute-done.2.refs_3_ = bf16[128,2048]{1,0:T(8,128)(2,1)} collective-permute-done((bf16[128,2048]{1,0:T(8,128)(2,1)}, bf16[128,2048]{1,0:T(8,128)(2,1)}, u32[]{:S(2)}, u32[]{:S(2)}) %collective-permute-start.2) | collective-permute-done | bytes 524320 | tf_op jit(solution)/shard_map/ppermute | solution.py:45
  62.6 2.9 %collective-permute-start.6 = (bf16[128,2048]{1,0:T(8,128)(2,1)}, bf16[128,2048]{1,0:T(8,128)(2,1)}, u32[]{:S(2)}, u32[]{:S(2)}) collective-permute-start(bf16[128,2048]{1,0:T(8,128)(2,1)} %collective-permute-done.2.refs_3_), channel_id=1, source_target_pairs={{0,1},{1,0},{2,3},{3,2},{4,5},{5,4},{6,7},{7,6},{8,9},{9,8},{10,11... | collective-permute-start | bytes 1572872 | tf_op jit(solution)/shard_map/ppermute | solution.py:49
  65.6 3.2 %collective-permute-done.refs_1_ = bf16[128,2048]{1,0:T(8,128)(2,1)} collective-permute-done((bf16[128,2048]{1,0:T(8,128)(2,1)}, bf16[128,2048]{1,0:T(8,128)(2,1)}, u32[]{:S(2)}, u32[]{:S(2)}) %collective-permute-start) | collective-permute-done | bytes 524320 | tf_op jit(solution)/shard_map/ppermute | solution.py:45
  68.8 2.4 %collective-permute-start.4 = (bf16[128,2048]{1,0:T(8,128)(2,1)}, bf16[128,2048]{1,0:T(8,128)(2,1)}, u32[]{:S(2)}, u32[]{:S(2)}) collective-permute-start(bf16[128,2048]{1,0:T(8,128)(2,1)} %collective-permute-done.refs_1_), channel_id=1, source_target_pairs={{0,1},{1,0},{2,3},{3,2},{4,5},{5,4},{6,7},{7,6},{8,9},{9,8},{10,11... | collective-permute-start | bytes 1572872 | tf_op jit(solution)/shard_map/ppermute | solution.py:49
  71.2 1.9 %collective-permute-start.5 = (bf16[128,2048]{1,0:T(8,128)(2,1)}, bf16[128,2048]{1,0:T(8,128)(2,1)}, u32[]{:S(2)}, u32[]{:S(2)}) collective-permute-start(bf16[128,2048]{1,0:T(8,128)(2,1)} %collective-permute-done.1.refs_2_), channel_id=1, source_target_pairs={{0,1},{1,0},{2,3},{3,2},{4,5},{5,4},{6,7},{7,6},{8,9},{9,8},{10,11... | collective-permute-start | bytes 1572872 | tf_op jit(solution)/shard_map/ppermute | solution.py:49
  73.3 2.0 %collective-permute-done.5.refs_6_ = bf16[128,2048]{1,0:T(8,128)(2,1)} collective-permute-done((bf16[128,2048]{1,0:T(8,128)(2,1)}, bf16[128,2048]{1,0:T(8,128)(2,1)}, u32[]{:S(2)}, u32[]{:S(2)}) %collective-permute-start.5) | collective-permute-done | bytes 524320 | tf_op jit(solution)/shard_map/ppermute | solution.py:49
  76.4 6.3 %shard_map.92 = (bf16[1024,128]{1,0:T(8,128)(2,1)}, bf16[1024,128]{1,0:T(8,128)(2,1)}, bf16[1024,128]{1,0:T(8,128)(2,1)}, bf16[8,128,128]{2,1,0:T(8,128)(2,1)}, ...) custom-call(s32[4]{0:T(128)S(1)} %pad_add_fusion.place, f32[8,1]{1,0:T(8,128)S(1)} %copy.12.rates, ...), custom_call_target="tpu_custom_call" | custom-call | flops 1700000000 | bytes 7340032 | tf_op jit(solution)/shard_map/pallas_call | solution.py:245
  82.7 2.4 %collective-permute-start.9 = (bf16[2048,128]{1,0:T(8,128)(2,1)}, bf16[2048,128]{1,0:T(8,128)(2,1)S(1)}, u32[]{:S(2)}, u32[]{:S(2)}) collective-permute-start(bf16[2048,128]{1,0:T(8,128)(2,1)} %bitcast.14), channel_id=1, source_target_pairs={{0,6},{2,0},{4,2},{6,4},{1,7},{3,1},{5,3},{7,5},{8,14},{10,8},{12,... | collective-permute-start | bytes 1572872 | tf_op jit(solution)/shard_map/ppermute | solution.py:45
  85.0 2.4 %collective-permute-start.8 = (bf16[2048,128]{1,0:T(8,128)(2,1)}, bf16[2048,128]{1,0:T(8,128)(2,1)S(1)}, u32[]{:S(2)}, u32[]{:S(2)}) collective-permute-start(bf16[2048,128]{1,0:T(8,128)(2,1)} %bitcast.15), channel_id=1, source_target_pairs={{0,4},{2,6},{4,0},{6,2},{1,5},{3,7},{5,1},{7,3},{8,12},{10,14},{12... | collective-permute-start | bytes 1572872 | tf_op jit(solution)/shard_map/ppermute | solution.py:45
  87.5 2.5 %collective-permute-start.7 = (bf16[2048,128]{1,0:T(8,128)(2,1)}, bf16[2048,128]{1,0:T(8,128)(2,1)S(1)}, u32[]{:S(2)}, u32[]{:S(2)}) collective-permute-start(bf16[2048,128]{1,0:T(8,128)(2,1)} %bitcast.16), channel_id=1, source_target_pairs={{0,2},{2,4},{4,6},{6,0},{1,3},{3,5},{5,7},{7,1},{8,10},{10,12},{12... | collective-permute-start | bytes 1572872 | tf_op jit(solution)/shard_map/ppermute | solution.py:45
  90.0 8.2 %collective-permute-done.9.refs_3_ = bf16[2048,128]{1,0:T(8,128)(2,1)S(1)} collective-permute-done((bf16[2048,128]{1,0:T(8,128)(2,1)}, bf16[2048,128]{1,0:T(8,128)(2,1)S(1)}, u32[]{:S(2)}, u32[]{:S(2)}) %collective-permute-start.9) | collective-permute-done | bytes 524320 | tf_op jit(solution)/shard_map/ppermute | solution.py:45
  98.2 3.5 %collective-permute-done.8.refs_2_ = bf16[2048,128]{1,0:T(8,128)(2,1)S(1)} collective-permute-done((bf16[2048,128]{1,0:T(8,128)(2,1)}, bf16[2048,128]{1,0:T(8,128)(2,1)S(1)}, u32[]{:S(2)}, u32[]{:S(2)}) %collective-permute-start.8) | collective-permute-done | bytes 524320 | tf_op jit(solution)/shard_map/ppermute | solution.py:45
  101.7 12.0 %collective-permute-done.7.refs_1_ = bf16[2048,128]{1,0:T(8,128)(2,1)S(1)} collective-permute-done((bf16[2048,128]{1,0:T(8,128)(2,1)}, bf16[2048,128]{1,0:T(8,128)(2,1)S(1)}, u32[]{:S(2)}, u32[]{:S(2)}) %collective-permute-start.7) | collective-permute-done | bytes 524320 | tf_op jit(solution)/shard_map/ppermute | solution.py:45
  114.5 1.5 shard_map.96.same_ref
  116.1 2.4 %collective-permute-start.10 = (bf16[4,2048,128]{2,1,0:T(8,128)(2,1)S(1)}, bf16[4,2048,128]{2,1,0:T(8,128)(2,1)}, u32[]{:S(2)}, u32[]{:S(2)}) collective-permute-start(bf16[4,2048,128]{2,1,0:T(8,128)(2,1)S(1)} %shard_map.96.same_ref), channel_id=1, source_target_pairs={{0,1},{1,0},{2,3},{3,2},{4,5},{5,4},{6,7},{7,6},{8,9},{9,8},{10,11... | collective-permute-start | bytes 6291464 | tf_op jit(solution)/shard_map/ppermute | solution.py:49
  118.5 16.7 %all_to_all.26.got = bf16[8,136,128]{2,1,0:T(8,128)(2,1)S(1)} all-to-all(bf16[8,136,128]{2,1,0:T(8,128)(2,1)S(1)} %copy-done.5), channel_id=1, replica_groups=mesh['sp_0'=8,'sp_1'=8,'tp_0'=4,'tp_1'=2] {'sp_1'}, dimensions={0} | all-to-all | bytes 557056 | tf_op jit(solution)/shard_map/all_to_all | solution.py:474
  136.6 5.2 %all-to-all-start.3 = ((bf16[8,136,128]{2,1,0:T(8,128)(2,1)}), bf16[8,136,128]{2,1,0:T(8,128)(2,1)S(1)}, u32[]{:S(2)}, u32[]{:S(2)}) async-start(bf16[8,136,128]{2,1,0:T(8,128)(2,1)} %get-tuple-element.21), calls=%async_computation.3 | async-start | bytes 557056 | tf_op jit(solution)/shard_map/all_to_all | solution.py:476
  141.8 3.2 %shard_map.94.l_hbm = bf16[1024,128]{1,0:T(8,128)(2,1)} custom-call(f32[8,1]{1,0:T(8,128)S(1)} %copy.12.rates, bf16[1024,128]{1,0:T(8,128)(2,1)} %get-tuple-element.24.q_hbm, bf16[1024,128]{1,0:T(8,128)(2,1)} %get-tuple-element.25.k_hbm, bf16[1024,128]{1,0:T(8,128)(2,1)} %get-tuple-element.26.v_hbm, bf16[8,128,128]{2,1,0:T(8,128)(2,1)} %get-tuple-element.27.p_hbm), custom_call_target="tpu_custom_call" | custom-call | flops 1000000000 | bytes 2097152 | tf_op jit(solution)/shard_map/pallas_call | solution.py:305
  145.0 7.9 %all-to-all-done.3.got = bf16[8,136,128]{2,1,0:T(8,128)(2,1)S(1)} async-done(((bf16[8,136,128]{2,1,0:T(8,128)(2,1)}), bf16[8,136,128]{2,1,0:T(8,128)(2,1)S(1)}, u32[]{:S(2)}, u32[]{:S(2)}) %all-to-all-start.3) | async-done | bytes 278560 | tf_op jit(solution)/shard_map/all_to_all | solution.py:476
  152.9 2.1 %shard_map.95 = bf16[8,128,128]{2,1,0:T(8,128)(2,1)S(1)} custom-call(s32[4]{0:T(128)S(1)} %pad_add_fusion.place, f32[8,1]{1,0:T(8,128)S(1)} %copy.12.rates, bf16[8,136,128]{2,1,0:T(8,128)(2,1)S(1)} %all-to-all-done.3.got, f32[128,128]{1,0:T(8,128)S(1)} %get-tuple-element.22.before_ref, f32[8,128]{1,0:T(8,128)S(1)} %get-tuple-element.23.shrunk_ref, ...), custom_call_target="tpu_custom_call" | custom-call | flops 40000000 | bytes 1048576 | tf_op jit(solution)/shard_map/pallas_call | solution.py:379
  155.0 11.0 %all_to_all.27.h_ref = bf16[8,128,128]{2,1,0:T(8,128)(2,1)S(1)} all-to-all(bf16[8,128,128]{2,1,0:T(8,128)(2,1)S(1)} %shard_map.95), channel_id=1, replica_groups=mesh['sp_0'=8,'sp_1'=8,'tp_0'=4,'tp_1'=2] {'tp_0','tp_1'}, dimensions={0} | all-to-all | bytes 524288 | tf_op jit(solution)/shard_map/all_to_all | solution.py:488
  167.2 3.3 %shard_map.98 = bf16[128,2048]{1,0:T(8,128)(2,1)} custom-call(s32[4]{0:T(128)S(1)} %pad_add_fusion.place, bf16[8,128,128]{2,1,0:T(8,128)(2,1)S(1)} %all_to_all.27.h_ref, f32[128,2048]{1,0:T(8,128)S(1)} %shard_map.97.partial_ref, bf16[4,2048,128]{2,1,0:T(8,128)(2,1)} %collective-permute-done.10.other_hbm), custom_call_target="tpu_custom_call" | custom-call | flops 270000000 | bytes 4194304 | tf_op jit(solution)/shard_map/pallas_call | solution.py:432
  (28 shorter events, 5.8 us)
Async XLA Ops:
  22.3 53.0 %all-to-all-start.1 = ((bf16[8,256,512]{2,1,0:T(8,128)(2,1)}), bf16[8,256,512]{2,1,0:T(8,128)(2,1)S(1)}, u32[]{:S(2)}, u32[]{:S(2)}) async-start(bf16[8,256,512]{2,1,0:T(8,128)(2,1)} %broadcast_in_dim.24), calls=%async_computation.1 | async-start | bytes 4194304 | tf_op jit(solution)/shard_map/all_to_all | solution.py:40
  31.3 42.0 %collective-permute-start.3 = (bf16[128,2048]{1,0:T(8,128)(2,1)}, bf16[128,2048]{1,0:T(8,128)(2,1)}, u32[]{:S(2)}, u32[]{:S(2)}) collective-permute-start(bf16[128,2048]{1,0:T(8,128)(2,1)} %shard_map.91.refs_0_), channel_id=1, source_target_pairs={{0,1},{1,0},{2,3},{3,2},{4,5},{5,4},{6,7},{7,6},{8,9},{9,8},{10,11... | collective-permute-start | bytes 1572872 | tf_op jit(solution)/shard_map/ppermute | solution.py:49
  35.6 27.0 %collective-permute-start.2 = (bf16[128,2048]{1,0:T(8,128)(2,1)}, bf16[128,2048]{1,0:T(8,128)(2,1)}, u32[]{:S(2)}, u32[]{:S(2)}) collective-permute-start(bf16[128,2048]{1,0:T(8,128)(2,1)} %shard_map.91.refs_0_), channel_id=1, source_target_pairs={{0,6},{2,0},{4,2},{6,4},{1,7},{3,1},{5,3},{7,5},{8,14},{10,8},{12,... | collective-permute-start | bytes 1572872 | tf_op jit(solution)/shard_map/ppermute | solution.py:45
  40.0 16.9 %collective-permute-start.1 = (bf16[128,2048]{1,0:T(8,128)(2,1)}, bf16[128,2048]{1,0:T(8,128)(2,1)}, u32[]{:S(2)}, u32[]{:S(2)}) collective-permute-start(bf16[128,2048]{1,0:T(8,128)(2,1)} %shard_map.91.refs_0_), channel_id=1, source_target_pairs={{0,4},{2,6},{4,0},{6,2},{1,5},{3,7},{5,1},{7,3},{8,12},{10,14},{12... | collective-permute-start | bytes 1572872 | tf_op jit(solution)/shard_map/ppermute | solution.py:45
  42.4 26.4 %collective-permute-start = (bf16[128,2048]{1,0:T(8,128)(2,1)}, bf16[128,2048]{1,0:T(8,128)(2,1)}, u32[]{:S(2)}, u32[]{:S(2)}) collective-permute-start(bf16[128,2048]{1,0:T(8,128)(2,1)} %shard_map.91.refs_0_), channel_id=1, source_target_pairs={{0,2},{2,4},{4,6},{6,0},{1,3},{3,5},{5,7},{7,1},{8,10},{10,12},{12... | collective-permute-start | bytes 1572872 | tf_op jit(solution)/shard_map/ppermute | solution.py:45
  45.0 28.1 %copy-start.6 = (f32[8,1]{0,1:T(1,128)S(1)}, f32[8,1]{0,1:T(1,128)}, u32[]{:S(2)}) copy-start(f32[8,1]{0,1:T(1,128)} %param.14) | copy-start | bytes 100
  62.6 10.7 %collective-permute-start.6 = (bf16[128,2048]{1,0:T(8,128)(2,1)}, bf16[128,2048]{1,0:T(8,128)(2,1)}, u32[]{:S(2)}, u32[]{:S(2)}) collective-permute-start(bf16[128,2048]{1,0:T(8,128)(2,1)} %collective-permute-done.2.refs_3_), channel_id=1, source_target_pairs={{0,1},{1,0},{2,3},{3,2},{4,5},{5,4},{6,7},{7,6},{8,9},{9,8},{10,11... | collective-permute-start | bytes 1572872 | tf_op jit(solution)/shard_map/ppermute | solution.py:49
  68.8 4.5 %collective-permute-start.4 = (bf16[128,2048]{1,0:T(8,128)(2,1)}, bf16[128,2048]{1,0:T(8,128)(2,1)}, u32[]{:S(2)}, u32[]{:S(2)}) collective-permute-start(bf16[128,2048]{1,0:T(8,128)(2,1)} %collective-permute-done.refs_1_), channel_id=1, source_target_pairs={{0,1},{1,0},{2,3},{3,2},{4,5},{5,4},{6,7},{7,6},{8,9},{9,8},{10,11... | collective-permute-start | bytes 1572872 | tf_op jit(solution)/shard_map/ppermute | solution.py:49
  71.2 4.1 %collective-permute-start.5 = (bf16[128,2048]{1,0:T(8,128)(2,1)}, bf16[128,2048]{1,0:T(8,128)(2,1)}, u32[]{:S(2)}, u32[]{:S(2)}) collective-permute-start(bf16[128,2048]{1,0:T(8,128)(2,1)} %collective-permute-done.1.refs_2_), channel_id=1, source_target_pairs={{0,1},{1,0},{2,3},{3,2},{4,5},{5,4},{6,7},{7,6},{8,9},{9,8},{10,11... | collective-permute-start | bytes 1572872 | tf_op jit(solution)/shard_map/ppermute | solution.py:49
  75.3 1.0 copy-start
  82.6 35.8 %copy-start.5 = (bf16[8,136,128]{2,1,0:T(8,128)(2,1)S(1)}, bf16[8,136,128]{2,1,0:T(8,128)(2,1)}, u32[]{:S(2)}) copy-start(bf16[8,136,128]{2,1,0:T(8,128)(2,1)} %get-tuple-element.20) | copy-start | bytes 835588
  82.7 15.6 %collective-permute-start.9 = (bf16[2048,128]{1,0:T(8,128)(2,1)}, bf16[2048,128]{1,0:T(8,128)(2,1)S(1)}, u32[]{:S(2)}, u32[]{:S(2)}) collective-permute-start(bf16[2048,128]{1,0:T(8,128)(2,1)} %bitcast.14), channel_id=1, source_target_pairs={{0,6},{2,0},{4,2},{6,4},{1,7},{3,1},{5,3},{7,5},{8,14},{10,8},{12,... | collective-permute-start | bytes 1572872 | tf_op jit(solution)/shard_map/ppermute | solution.py:45
  85.0 16.7 %collective-permute-start.8 = (bf16[2048,128]{1,0:T(8,128)(2,1)}, bf16[2048,128]{1,0:T(8,128)(2,1)S(1)}, u32[]{:S(2)}, u32[]{:S(2)}) collective-permute-start(bf16[2048,128]{1,0:T(8,128)(2,1)} %bitcast.15), channel_id=1, source_target_pairs={{0,4},{2,6},{4,0},{6,2},{1,5},{3,7},{5,1},{7,3},{8,12},{10,14},{12... | collective-permute-start | bytes 1572872 | tf_op jit(solution)/shard_map/ppermute | solution.py:45
  87.5 26.3 %collective-permute-start.7 = (bf16[2048,128]{1,0:T(8,128)(2,1)}, bf16[2048,128]{1,0:T(8,128)(2,1)S(1)}, u32[]{:S(2)}, u32[]{:S(2)}) collective-permute-start(bf16[2048,128]{1,0:T(8,128)(2,1)} %bitcast.16), channel_id=1, source_target_pairs={{0,2},{2,4},{4,6},{6,0},{1,3},{3,5},{5,7},{7,1},{8,10},{10,12},{12... | collective-permute-start | bytes 1572872 | tf_op jit(solution)/shard_map/ppermute | solution.py:45
  98.2 15.5 %copy-start.2 = (bf16[2048,128]{1,0:T(8,128)(2,1)}, bf16[2048,128]{1,0:T(8,128)(2,1)S(1)}, u32[]{:S(2)}) copy-start(bf16[2048,128]{1,0:T(8,128)(2,1)S(1)} %collective-permute-done.9.refs_3_) | copy-start | bytes 1572868
  101.7 12.0 %copy-start.3 = (bf16[2048,128]{1,0:T(8,128)(2,1)}, bf16[2048,128]{1,0:T(8,128)(2,1)S(1)}, u32[]{:S(2)}) copy-start(bf16[2048,128]{1,0:T(8,128)(2,1)S(1)} %collective-permute-done.8.refs_2_) | copy-start | bytes 1572868
  113.7 0.8 copy-start.4
  116.1 51.2 %collective-permute-start.10 = (bf16[4,2048,128]{2,1,0:T(8,128)(2,1)S(1)}, bf16[4,2048,128]{2,1,0:T(8,128)(2,1)}, u32[]{:S(2)}, u32[]{:S(2)}) collective-permute-start(bf16[4,2048,128]{2,1,0:T(8,128)(2,1)S(1)} %shard_map.96.same_ref), channel_id=1, source_target_pairs={{0,1},{1,0},{2,3},{3,2},{4,5},{5,4},{6,7},{7,6},{8,9},{9,8},{10,11... | collective-permute-start | bytes 6291464 | tf_op jit(solution)/shard_map/ppermute | solution.py:49
  136.6 16.3 %copy-start.1 = (f32[128]{0:T(128)S(1)}, f32[128]{0:T(128)}, u32[]{:S(2)}) copy-start(f32[128]{0:T(128)} %param.16) | copy-start | bytes 1540
  136.6 16.3 %all-to-all-start.3 = ((bf16[8,136,128]{2,1,0:T(8,128)(2,1)}), bf16[8,136,128]{2,1,0:T(8,128)(2,1)S(1)}, u32[]{:S(2)}, u32[]{:S(2)}) async-start(bf16[8,136,128]{2,1,0:T(8,128)(2,1)} %get-tuple-element.21), calls=%async_computation.3 | async-start | bytes 557056 | tf_op jit(solution)/shard_map/all_to_all | solution.py:476
